TPU v7x, 256 devices: a whole 4x4x8 slice. The times are simulated.
256 devices in a mesh: sp: 16 (over y, x), tp: 16 (over z, core).
Axes of the slice: x: 4, y: 4, z: 8, core: 2. Of those that a mesh axis runs over, the one named last changes fastest.
Arguments:
- conv_in: bfloat16 [1024, 65536], P('tp', 'sp'), may hold values from -6 to 6
- in_gate: bfloat16 [1024, 65536], P('tp', 'sp'), may hold values from -6 to 6
- out_gate: bfloat16 [1024, 65536], P('tp', 'sp'), may hold values from -6 to 6
- doc_ids: int32 [65536], P('sp'), may hold values from 0 to 7, never falling along the last dimension, each value on 1 to 12288 neighbouring positions
- conv_taps: float32 [1024, 3], P('tp'), may hold values from -3.5 to 3.5
- head_gain: float32 [1024], P('tp'), may hold values from 0.1 to 1.9
- out_proj: bfloat16 [1024, 2048], P('tp'), may hold values from -0.1875 to 0.1875
- resid: bfloat16 [65536, 2048], P(('sp', 'tp')), may hold values from -6 to 6
- norm_gain: float32 [2048], replicated, may hold values from 0.1 to 1.9
- route_ids: int32 [65536, 2], P(('sp', 'tp')), may hold values from 0 to 15, all different within a row; in each aligned block of 128 rows (0 to 127, 128 to 255, ...) at most 32 rows name the same one
- route_weight: float32 [65536, 2], P(('sp', 'tp')), may hold values from 0.1 to 1
- w_gate: bfloat16 [16, 2048, 512], P('sp'), may hold values from -0.125 to 0.125
- w_up: bfloat16 [16, 2048, 512], P('sp'), may hold values from -0.125 to 0.125
- w_down: bfloat16 [16, 512, 2048], P('sp'), may hold values from -0.25 to 0.25
Outputs:
- layer_out: bfloat16 [65536, 2048], P(('sp', 'tp'))
Inputs may be any that keep to these rules, and one draw needn't show every extreme that they name: `doc_ids`: document numbers never fall along the sequence; every number from 0 to 7 is used; no document is longer than 12288 positions and one is exactly that long. `route_ids`: each position names 2 different experts. In every aligned block of 128 positions no expert is named by more than 32 positions, a bound that some block reaches.
All inputs are finite; a program needn't handle non-finite values.
Results may differ from a plain program's by a relative error of at most 0.0051.
Values may be sent and summed in bfloat16 or wider, within the bound.
A program may use at most 64 MiB of HBM per device.

v0:
```python
import jax
import jax.numpy as jnp
from jax import lax
from jax.sharding import Mesh
from jax.sharding import PartitionSpec as P

HEAD = 64
TP = ("tp_0", "tp_1")
SP_TP = ("sp", "tp_0", "tp_1")


norm_eps = 1e-06


def shifted(value, axis, steps):
    count = lax.axis_size(axis)
    leading, last = (max(0, -steps), min(count, count - steps))
    return lax.ppermute(value, axis, [(source, source + steps) for source in range(leading, last)])


def cut_along(array, dim, length):
    before, after = (array.shape[:dim], array.shape[dim + 1 :])
    return jnp.moveaxis(array.reshape(*before, length, -1, *after), dim, 0)


def joined_along(pieces, dim):
    dims = list(pieces.shape[1:])
    dims[dim] *= pieces.shape[0]
    return jnp.moveaxis(pieces, 0, dim).reshape(dims)


def exchange_in_order(pieces, axes, sequence):
    dims = [lax.axis_size(a) for a in axes]
    pieces = pieces.reshape(*dims, *pieces.shape[1:])
    for k in sequence:
        pieces = lax.all_to_all(pieces, axes[k], split_axis=k, concat_axis=k, tiled=True)
    return pieces.reshape(-1, *pieces.shape[len(axes) :])


def exchange_by_chip(array, groups, sequence, split_dim, concat_dim):
    length = lax.axis_size(groups[0]) * lax.axis_size(groups[1])
    pieces = cut_along(array, split_dim, length)
    return joined_along(exchange_in_order(pieces, groups, sequence), concat_dim)


def slot_places(ids_block, slot, experts):
    flat = ids_block.reshape(-1)
    marks = (flat[:, None] == jnp.arange(experts, dtype=jnp.int32)[None, :]).astype(jnp.int32)
    before = jnp.sum((jnp.cumsum(marks, axis=0) - 1) * marks, axis=1)
    return (flat * slot + before).reshape(ids_block.shape)


def pack_rows(places, normed_rows, total_slots):
    targets = jnp.arange(total_slots, dtype=jnp.int32)
    table = jnp.any(targets[:, None, None] == places[None, :, :], axis=2).astype(jnp.bfloat16)
    return jnp.dot(table, normed_rows, preferred_element_type=jnp.float32).astype(jnp.bfloat16)


def combine_rows(returned, places, weights):
    totals = jnp.zeros((places.shape[0], returned.shape[1]), jnp.float32)
    for choice_k in range(places.shape[1]):
        totals = totals + weights[:, choice_k : choice_k + 1] * returned[
            places[:, choice_k]
        ].astype(jnp.float32)
    return totals


def body(
    conv_in,
    in_gate,
    out_gate,
    doc_ids,
    conv_taps,
    head_gain,
    out_proj,
    resid,
    norm_gain,
    route_ids,
    route_weight,
    w_gate,
    w_up,
    w_down,
):
    gated_in = in_gate.astype(jnp.float32) * conv_in.astype(jnp.float32)
    doc_value = doc_ids.astype(jnp.float32)
    earlier_in, earlier_doc = shifted((gated_in[:, -2:], doc_value[-2:]), "sp", 1)
    padded_in = jnp.concatenate([earlier_in, gated_in], axis=1)
    padded_doc = jnp.concatenate([earlier_doc, doc_value])
    same_one = (padded_doc[1:-1] == doc_value).astype(jnp.float32)
    same_two = (padded_doc[:-2] == doc_value).astype(jnp.float32)
    conv_out = (
        conv_taps[:, 2:3] * gated_in
        + conv_taps[:, 1:2] * (padded_in[:, 1:-1] * same_one)
        + conv_taps[:, 0:1] * (padded_in[:, :-2] * same_two)
    )
    gated_out = out_gate.astype(jnp.float32) * conv_out
    channels = gated_out.shape[0]
    by_head = gated_out.reshape(channels // HEAD, HEAD, -1)
    by_head = by_head * lax.rsqrt(jnp.mean(by_head * by_head, axis=1, keepdims=True) + norm_eps)
    head_normed = (by_head.reshape(channels, -1) * head_gain[:, None]).astype(jnp.bfloat16)
    by_row = exchange_by_chip(head_normed, ("tp_0", "tp_1"), (0, 1), 1, 0)
    rows = resid.shape[0]
    width = resid.shape[1]
    mixed = lax.dot_general(
        by_row,
        lax.all_gather(out_proj, TP, axis=0, tiled=True),
        (((0,), (0,)), ((), ())),
        preferred_element_type=jnp.float32,
    )
    stream = resid.astype(jnp.float32) + mixed
    expert_in = (
        stream * lax.rsqrt(jnp.mean(stream * stream, axis=1, keepdims=True) + norm_eps) * norm_gain
    ).astype(jnp.bfloat16)
    sp_count = lax.axis_size("sp")
    local_experts = w_gate.shape[0]
    experts_total = local_experts * sp_count
    half = rows // 2
    slot = max(2, rows // 8)
    parts = []
    for block_no in range(2):
        block_ids = route_ids[block_no * half : (block_no + 1) * half]
        place = slot_places(block_ids, slot, experts_total)
        send = pack_rows(
            place, expert_in[block_no * half : (block_no + 1) * half], experts_total * slot
        ).reshape(sp_count, local_experts, slot, width)
        arrived = lax.all_to_all(send, "sp", split_axis=0, concat_axis=0, tiled=True)
        gate_part = jnp.einsum(
            "nesd,edf->nesf", arrived, w_gate, preferred_element_type=jnp.float32
        )
        up_part = jnp.einsum("nesd,edf->nesf", arrived, w_up, preferred_element_type=jnp.float32)
        hidden = (jax.nn.silu(gate_part) * up_part).astype(jnp.bfloat16)
        arrived = jnp.einsum(
            "nesf,efd->nesd", hidden, w_down, preferred_element_type=jnp.float32
        ).astype(jnp.bfloat16)
        returned = lax.all_to_all(arrived, "sp", split_axis=0, concat_axis=0, tiled=True).reshape(
            experts_total * slot, width
        )
        parts.append(
            combine_rows(returned, place, route_weight[block_no * half : (block_no + 1) * half])
        )
    mixture = jnp.concatenate(parts, axis=0)
    return (stream + mixture).astype(jnp.bfloat16)


def solution(mesh):
    finer = Mesh(mesh.devices.reshape(mesh.shape["sp"], 8, 2), ("sp", "tp_0", "tp_1"))
    return jax.shard_map(
        body,
        mesh=finer,
        in_specs=(
            P(TP, "sp"),
            P(TP, "sp"),
            P(TP, "sp"),
            P("sp"),
            P(TP, None),
            P(TP),
            P(TP, None),
            P(SP_TP, None),
            P(),
            P(SP_TP, None),
            P(SP_TP, None),
            P("sp", None, None),
            P("sp", None, None),
            P("sp", None, None),
        ),
        out_specs=P(SP_TP, None),
        check_vma=False,
    )
```

profile of v0, /device:TPU:32, one launch (start us, length us, event | category | flops | bytes accessed | tf_op | source)
XLA Modules:
  0.0 229.9 jit_solution(15386730923567032720)
XLA Ops:
  6.5 0.7 all-gather.2.cloned.1.call-update
  7.3 0.8 convert_element_type.95
  8.1 3.4 %collective-permute-start.1 = (f32[2]{0:T(128)S(1)}, f32[2]{0:T(128)S(1)}, u32[]{:S(2)}, u32[]{:S(2)}) collective-permute-start(f32[2]{0:T(128)S(1)} %slice.117), channel_id=1, source_target_pairs={{0,16},{16,32},{32,48},{48,64},{64,80},{80,96},{96,112},{112,128},... | collective-permute-start | bytes 32 | tf_op jit(solution)/shard_map/ppermute | solution.py:18
  11.5 1.3 convert_multiply_fusion
  12.9 3.4 %collective-permute-start = (f32[64,2]{1,0:T(8,128)S(1)}, f32[64,2]{1,0:T(8,128)S(1)}, u32[]{:S(2)}, u32[]{:S(2)}) collective-permute-start(f32[64,2]{1,0:T(8,128)S(1)} %slice.114), channel_id=1, source_target_pairs={{0,16},{16,32},{32,48},{48,64},{64,80},{80,96},{96,112},{112,128},... | collective-permute-start | bytes 1544 | tf_op jit(solution)/shard_map/ppermute | solution.py:18
  16.4 1.5 collective-permute-done
  19.4 1.0 copy.57
  20.3 8.6 %all-to-all-start = ((bf16[8,2,64,256]{3,2,1,0:T(8,128)(2,1)}), bf16[8,2,64,256]{3,2,1,0:T(8,128)(2,1)S(1)}, u32[]{:S(2)}, u32[]{:S(2)}) async-start(bf16[8,2,64,256]{3,2,1,0:T(8,128)(2,1)} %bitcast.4), calls=%async_computation | async-start | bytes 1048576 | tf_op jit(solution)/shard_map/all_to_all | solution.py:36
  30.5 20.4 %all-to-all-done = bf16[8,2,64,256]{3,2,1,0:T(8,128)(2,1)S(1)} async-done(((bf16[8,2,64,256]{3,2,1,0:T(8,128)(2,1)}), bf16[8,2,64,256]{3,2,1,0:T(8,128)(2,1)S(1)}, u32[]{:S(2)}, u32[]{:S(2)}) %all-to-all-start) | async-done | bytes 524320 | tf_op jit(solution)/shard_map/all_to_all | solution.py:36
  51.0 4.2 %all_to_all.30 = bf16[8,2,64,256]{3,2,0,1:T(8,128)(2,1)S(1)} all-to-all(bf16[8,2,64,256]{3,2,0,1:T(8,128)(2,1)S(1)} %copy.58), channel_id=1, replica_groups=mesh['sp'=16,'tp_0'=8,'tp_1'=2] {'tp_1'}, dimensions={1} | all-to-all | bytes 1048576 | tf_op jit(solution)/shard_map/all_to_all | solution.py:36
  55.3 7.1 %all-gather.2.cloned.1.call-done = bf16[1024,2048]{1,0:T(8,128)(2,1)} async-done(((bf16[64,2048]{1,0:T(8,128)(2,1)}), bf16[1024,2048]{1,0:T(8,128)(2,1)}) %all-gather.2.cloned.1.call-update) | async-done | bytes 4194320 | tf_op jit(solution)/shard_map/all_gather | solution.py:106
  62.4 3.9 %multiply_reduce_fusion = (f32[256]{0:T(256)S(1)}, f32[256,2048]{1,0:T(8,128)S(1)}) fusion(bf16[1024,256]{1,0:T(8,128)(2,1)S(1)} %bitcast.207, bf16[1024,2048]{1,0:T(8,128)(2,1)} %all-gather.2.cloned.1.call-done, bf16[256,2048]{1,0:T(8,128)(2,1)} %param.21), kind=kOutput, calls=%fused_computation.28 | convolution fusion | flops 1075838720 | bytes 7865344 | tf_op jit(solution)/shard_map/dot_general | solution.py:104
  66.6 2.0 convolution_convert_fusion.3
  68.6 6.9 %all-to-all-start.2 = ((bf16[16,1,32,2048]{3,2,1,0:T(8,128)(2,1)}), bf16[16,1,32,2048]{3,2,1,0:T(8,128)(2,1)}, u32[]{:S(2)}, u32[]{:S(2)}) async-start(bf16[16,1,32,2048]{3,2,1,0:T(8,128)(2,1)} %bitcast.204), calls=%async_computation.2 | async-start | bytes 4194304 | tf_op jit(solution)/shard_map/all_to_all | solution.py:126
  77.1 2.1 convolution_convert_fusion.1
  79.2 29.7 %all-to-all-done.2 = bf16[16,1,32,2048]{3,2,1,0:T(8,128)(2,1)} async-done(((bf16[16,1,32,2048]{3,2,1,0:T(8,128)(2,1)}), bf16[16,1,32,2048]{3,2,1,0:T(8,128)(2,1)}, u32[]{:S(2)}, u32[]{:S(2)}) %all-to-all-start.2) | async-done | bytes 2097184 | tf_op jit(solution)/shard_map/all_to_all | solution.py:126
  108.9 4.4 %all-to-all-start.4 = ((bf16[16,1,32,2048]{3,2,1,0:T(8,128)(2,1)}), bf16[16,1,32,2048]{3,2,1,0:T(8,128)(2,1)}, u32[]{:S(2)}, u32[]{:S(2)}) async-start(bf16[16,1,32,2048]{3,2,1,0:T(8,128)(2,1)} %bitcast.205), calls=%async_computation.4 | async-start | bytes 4194304 | tf_op jit(solution)/shard_map/all_to_all | solution.py:126
  113.3 3.5 %fusion.17 = f32[16,1,32,512]{3,2,0,1:T(8,128)S(1)} fusion(bf16[1,2048,512]{2,1,0:T(8,128)(2,1)} %param.25, bf16[16,1,32,2048]{3,2,1,0:T(8,128)(2,1)} %all-to-all-done.2), kind=kOutput, calls=%fused_computation.29 | convolution fusion | flops 1073741824 | bytes 5242880 | tf_op jit(solution)/shard_map/nesd,edf->nesf/dot_general | solution.py:127
  116.8 6.0 %fusion = bf16[16,1,32,2048]{3,2,1,0:T(8,128)(2,1)} fusion(bf16[1,512,2048]{2,1,0:T(8,128)(2,1)S(1)} %copy-done, bf16[1,2048,512]{2,1,0:T(8,128)(2,1)} %param.26, bf16[16,1,32,2048]{3,2,1,0:T(8,128)(2,1)} %all-to-all-done.2, f32[16,1,32,512]{3,2,0,1:T(8,128)S(1)} %fusion.17), kind=kOutput, calls=%fused_computation.8 | convolution fusion | flops 2150105088 | bytes 9437184 | tf_op jit(solution)/shard_map/nesf,efd->nesd/dot_general | solution.py:132
  122.8 21.1 %all-to-all-done.4 = bf16[16,1,32,2048]{3,2,1,0:T(8,128)(2,1)} async-done(((bf16[16,1,32,2048]{3,2,1,0:T(8,128)(2,1)}), bf16[16,1,32,2048]{3,2,1,0:T(8,128)(2,1)}, u32[]{:S(2)}, u32[]{:S(2)}) %all-to-all-start.4) | async-done | bytes 2097184 | tf_op jit(solution)/shard_map/all_to_all | solution.py:126
  143.9 4.4 %all-to-all-start.3 = ((bf16[16,1,32,2048]{3,2,1,0:T(8,128)(2,1)}), bf16[16,1,32,2048]{3,2,1,0:T(8,128)(2,1)}, u32[]{:S(2)}, u32[]{:S(2)}) async-start(bf16[16,1,32,2048]{3,2,1,0:T(8,128)(2,1)} %fusion), calls=%async_computation.3 | async-start | bytes 4194304 | tf_op jit(solution)/shard_map/all_to_all | solution.py:135
  148.4 3.5 %fusion.32 = f32[16,1,32,512]{3,2,0,1:T(8,128)S(1)} fusion(bf16[1,2048,512]{2,1,0:T(8,128)(2,1)} %param.25, bf16[16,1,32,2048]{3,2,1,0:T(8,128)(2,1)} %all-to-all-done.4), kind=kOutput, calls=%fused_computation.32 | convolution fusion | flops 1073741824 | bytes 5242880 | tf_op jit(solution)/shard_map/nesd,edf->nesf/dot_general | solution.py:127
  151.9 6.1 %fusion.1 = bf16[16,1,32,2048]{3,2,1,0:T(8,128)(2,1)} fusion(bf16[1,512,2048]{2,1,0:T(8,128)(2,1)S(1)} %copy-done, bf16[1,2048,512]{2,1,0:T(8,128)(2,1)} %param.26, bf16[16,1,32,2048]{3,2,1,0:T(8,128)(2,1)} %all-to-all-done.4, f32[16,1,32,512]{3,2,0,1:T(8,128)S(1)} %fusion.32), kind=kOutput, calls=%fused_computation.9 | convolution fusion | flops 2150105088 | bytes 9437184 | tf_op jit(solution)/shard_map/nesf,efd->nesd/dot_general | solution.py:132
  157.9 20.1 %all-to-all-done.3 = bf16[16,1,32,2048]{3,2,1,0:T(8,128)(2,1)} async-done(((bf16[16,1,32,2048]{3,2,1,0:T(8,128)(2,1)}), bf16[16,1,32,2048]{3,2,1,0:T(8,128)(2,1)}, u32[]{:S(2)}, u32[]{:S(2)}) %all-to-all-start.3) | async-done | bytes 2097184 | tf_op jit(solution)/shard_map/all_to_all | solution.py:135
  178.1 4.6 %all-to-all-start.5 = ((bf16[16,1,32,2048]{3,2,1,0:T(8,128)(2,1)}), bf16[16,1,32,2048]{3,2,1,0:T(8,128)(2,1)}, u32[]{:S(2)}, u32[]{:S(2)}) async-start(bf16[16,1,32,2048]{3,2,1,0:T(8,128)(2,1)} %fusion.1), calls=%async_computation.5 | async-start | bytes 4194304 | tf_op jit(solution)/shard_map/all_to_all | solution.py:135
  183.1 3.3 %gather_fusion = bf16[128,2048]{1,0:T(8,128)(2,1)S(1)} fusion(bf16[512,2048]{1,0:T(8,128)(2,1)} %bitcast.30, s32[1024]{0:T(1024)S(1)} %get-tuple-element.27), kind=kCustom, calls=%fused_computation | custom fusion | bytes 1049088 | tf_op jit(solution)/shard_map/gather | solution.py:62
  186.4 3.3 %gather_fusion.1 = bf16[128,2048]{1,0:T(8,128)(2,1)S(1)} fusion(bf16[512,2048]{1,0:T(8,128)(2,1)} %bitcast.30, s32[1024]{0:T(1024)S(1)} %get-tuple-element.26), kind=kCustom, calls=%fused_computation.1 | custom fusion | bytes 1049088 | tf_op jit(solution)/shard_map/gather | solution.py:62
  189.7 21.9 %all-to-all-done.5 = bf16[16,1,32,2048]{3,2,1,0:T(8,128)(2,1)} async-done(((bf16[16,1,32,2048]{3,2,1,0:T(8,128)(2,1)}), bf16[16,1,32,2048]{3,2,1,0:T(8,128)(2,1)}, u32[]{:S(2)}, u32[]{:S(2)}) %all-to-all-start.5) | async-done | bytes 2097184 | tf_op jit(solution)/shard_map/all_to_all | solution.py:135
  211.7 4.1 %gather_fusion.2 = bf16[128,2048]{1,0:T(8,128)(2,1)} fusion(bf16[512,2048]{1,0:T(8,128)(2,1)} %bitcast.50, s32[1024]{0:T(1024)S(1)} %get-tuple-element.25), kind=kCustom, calls=%fused_computation.2 | custom fusion | bytes 1049088 | tf_op jit(solution)/shard_map/gather | solution.py:62
  215.8 4.1 %gather_fusion.3 = bf16[128,2048]{1,0:T(8,128)(2,1)} fusion(bf16[512,2048]{1,0:T(8,128)(2,1)} %bitcast.50, s32[1024]{0:T(1024)S(1)} %get-tuple-element.24), kind=kCustom, calls=%fused_computation.3 | custom fusion | bytes 1049088 | tf_op jit(solution)/shard_map/gather | solution.py:62
  220.1 0.8 copy-done.3
  221.8 1.2 fusion.2
  (70 shorter events, 6.7 us)
Async XLA Ops:
  6.5 110.3 %copy-start = (bf16[1,512,2048]{2,1,0:T(8,128)(2,1)S(1)}, bf16[1,512,2048]{2,1,0:T(8,128)(2,1)}, u32[]{:S(2)}) copy-start(bf16[1,512,2048]{2,1,0:T(8,128)(2,1)} %param.27) | copy-start | bytes 6291460
  6.5 9.8 %copy-start.9 = (f32[64,3]{0,1:T(4,128)S(1)}, f32[64,3]{0,1:T(4,128)}, u32[]{:S(2)}) copy-start(f32[64,3]{0,1:T(4,128)} %param.18) | copy-start | bytes 2308
  6.5 11.3 %copy-start.5 = (bf16[64,4096]{1,0:T(8,128)(2,1)S(1)}, bf16[64,4096]{1,0:T(8,128)(2,1)}, u32[]{:S(2)}) copy-start(bf16[64,4096]{1,0:T(8,128)(2,1)} %param.16) | copy-start | bytes 1572868
  6.5 55.9 %all-gather.2.cloned.1.call-start = ((), (), s32[]{:S(2)}) async-start(), calls=%async_computation.6 | async-start | bytes 4456448 | tf_op jit(solution)/shard_map/all_gather | solution.py:106
  8.1 8.2 %collective-permute-start.1 = (f32[2]{0:T(128)S(1)}, f32[2]{0:T(128)S(1)}, u32[]{:S(2)}, u32[]{:S(2)}) collective-permute-start(f32[2]{0:T(128)S(1)} %slice.117), channel_id=1, source_target_pairs={{0,16},{16,32},{32,48},{48,64},{64,80},{80,96},{96,112},{112,128},... | collective-permute-start | bytes 32 | tf_op jit(solution)/shard_map/ppermute | solution.py:18
  12.9 5.0 %collective-permute-start = (f32[64,2]{1,0:T(8,128)S(1)}, f32[64,2]{1,0:T(8,128)S(1)}, u32[]{:S(2)}, u32[]{:S(2)}) collective-permute-start(f32[64,2]{1,0:T(8,128)S(1)} %slice.114), channel_id=1, source_target_pairs={{0,16},{16,32},{32,48},{48,64},{64,80},{80,96},{96,112},{112,128},... | collective-permute-start | bytes 1544 | tf_op jit(solution)/shard_map/ppermute | solution.py:18
  18.6 0.7 copy-start.10
  19.2 9.7 %copy-start.7 = (s32[256,2]{0,1:T(2,128)S(1)}, s32[256,2]{0,1:T(2,128)}, u32[]{:S(2)}) copy-start(s32[256,2]{0,1:T(2,128)} %param.23) | copy-start | bytes 6148
  20.3 30.6 %all-to-all-start = ((bf16[8,2,64,256]{3,2,1,0:T(8,128)(2,1)}), bf16[8,2,64,256]{3,2,1,0:T(8,128)(2,1)S(1)}, u32[]{:S(2)}, u32[]{:S(2)}) async-start(bf16[8,2,64,256]{3,2,1,0:T(8,128)(2,1)} %bitcast.4), calls=%async_computation | async-start | bytes 1048576 | tf_op jit(solution)/shard_map/all_to_all | solution.py:36
  62.4 3.9 %copy-start.6 = (f32[2048]{0:T(1024)S(1)}, f32[2048]{0:T(1024)}, u32[]{:S(2)}) copy-start(f32[2048]{0:T(1024)} %param.22) | copy-start | bytes 24580
  66.3 2.3 copy-start.1
  68.6 40.3 %all-to-all-start.2 = ((bf16[16,1,32,2048]{3,2,1,0:T(8,128)(2,1)}), bf16[16,1,32,2048]{3,2,1,0:T(8,128)(2,1)}, u32[]{:S(2)}, u32[]{:S(2)}) async-start(bf16[16,1,32,2048]{3,2,1,0:T(8,128)(2,1)} %bitcast.204), calls=%async_computation.2 | async-start | bytes 4194304 | tf_op jit(solution)/shard_map/all_to_all | solution.py:126
  108.9 35.1 %all-to-all-start.4 = ((bf16[16,1,32,2048]{3,2,1,0:T(8,128)(2,1)}), bf16[16,1,32,2048]{3,2,1,0:T(8,128)(2,1)}, u32[]{:S(2)}, u32[]{:S(2)}) async-start(bf16[16,1,32,2048]{3,2,1,0:T(8,128)(2,1)} %bitcast.205), calls=%async_computation.4 | async-start | bytes 4194304 | tf_op jit(solution)/shard_map/all_to_all | solution.py:126
  143.9 34.1 %all-to-all-start.3 = ((bf16[16,1,32,2048]{3,2,1,0:T(8,128)(2,1)}), bf16[16,1,32,2048]{3,2,1,0:T(8,128)(2,1)}, u32[]{:S(2)}, u32[]{:S(2)}) async-start(bf16[16,1,32,2048]{3,2,1,0:T(8,128)(2,1)} %fusion), calls=%async_computation.3 | async-start | bytes 4194304 | tf_op jit(solution)/shard_map/all_to_all | solution.py:135
  157.9 25.2 %copy-start.8 = (f32[256,2]{0,1:T(2,128)S(1)}, f32[256,2]{0,1:T(2,128)}, u32[]{:S(2)}) copy-start(f32[256,2]{0,1:T(2,128)} %param.24) | copy-start | bytes 6148
  178.1 33.6 %all-to-all-start.5 = ((bf16[16,1,32,2048]{3,2,1,0:T(8,128)(2,1)}), bf16[16,1,32,2048]{3,2,1,0:T(8,128)(2,1)}, u32[]{:S(2)}, u32[]{:S(2)}) async-start(bf16[16,1,32,2048]{3,2,1,0:T(8,128)(2,1)} %fusion.1), calls=%async_computation.5 | async-start | bytes 4194304 | tf_op jit(solution)/shard_map/all_to_all | solution.py:135
  219.9 1.0 copy-start.3
  219.9 1.2 copy-start.4
  219.9 1.9 copy-start.2
Sparse Core Ops, SparseCore 0:
  9.2 53.2 all-gather.1
where the time goes:
time: 231 us; the launch traced here: 230 us
  waiting for transfers between devices  123 us (53%)
  starting transfers between devices  35.7 us (15%)
  matrix products  26.9 us (12%)
  local copies, waits for them, and re-layouts  19.6 us (8%)
  between operations  13.7 us (6%)
  other arithmetic  7 us (3%)
  blocking collectives  4.24 us (2%)
    all_to_all x2, waiting for transfers between devices, body(): lax.all_to_all(send, 'sp', split_axis=0, concat_axis=0, tiled=True)  50.8 us
    all_to_all x2, waiting for transfers between devices, body(): lax.all_to_all(arrived, 'sp', split_axis=0, concat_axis=0, tiled=True)  42.1 us
    all_to_all x1, waiting for transfers between devices, exchange_in_order(): lax.all_to_all(pieces, axes[k], split_axis=k, concat_axis=k, tiled=True)  20.4 us
    gather x4, local copies, waits for them, and re-layouts, combine_rows(): returned[places[:, choice_k]].astype(jnp.float32)  14.8 us
    dot_general x2, matrix products, body(): jnp.einsum('nesf,efd->nesd', hidden, w_down, preferred_element_type=jnp.f...  12.1 us
    all_to_all x2, starting transfers between devices, body(): lax.all_to_all(send, 'sp', split_axis=0, concat_axis=0, tiled=True)  11.3 us
    all_to_all x2, starting transfers between devices, body(): lax.all_to_all(arrived, 'sp', split_axis=0, concat_axis=0, tiled=True)  9.05 us
    all_to_all x1, starting transfers between devices, exchange_in_order(): lax.all_to_all(pieces, axes[k], split_axis=k, concat_axis=k, tiled=True)  8.57 us
  transfers between devices with their start and end apart: 8, of which 7 were waited for; matrix products, arithmetic and copies ran while one was open for 16% of the time, Pallas kernels for 0%

commit v1 on v0

--- a/solution.py
+++ b/solution.py
@@ -1,12 +1,17 @@
 import jax
 import jax.numpy as jnp
 from jax import lax
+from jax.experimental import pallas as pl
+from jax.experimental.pallas import tpu as pltpu
 from jax.sharding import Mesh
 from jax.sharding import PartitionSpec as P
 
 HEAD = 64
 TP = ("tp_0", "tp_1")
 SP_TP = ("sp", "tp_0", "tp_1")
+SIDE = 4
+PARTNERS = SIDE * SIDE
+BLOCKS = 2
 
 
 norm_eps = 1e-06
@@ -43,26 +48,211 @@
     return joined_along(exchange_in_order(pieces, groups, sequence), concat_dim)
 
 
-def slot_places(ids_block, slot, experts):
-    flat = ids_block.reshape(-1)
-    marks = (flat[:, None] == jnp.arange(experts, dtype=jnp.int32)[None, :]).astype(jnp.int32)
-    before = jnp.sum((jnp.cumsum(marks, axis=0) - 1) * marks, axis=1)
-    return (flat * slot + before).reshape(ids_block.shape)
-
-
-def pack_rows(places, normed_rows, total_slots):
-    targets = jnp.arange(total_slots, dtype=jnp.int32)
-    table = jnp.any(targets[:, None, None] == places[None, :, :], axis=2).astype(jnp.bfloat16)
-    return jnp.dot(table, normed_rows, preferred_element_type=jnp.float32).astype(jnp.bfloat16)
-
-
-def combine_rows(returned, places, weights):
-    totals = jnp.zeros((places.shape[0], returned.shape[1]), jnp.float32)
-    for choice_k in range(places.shape[1]):
-        totals = totals + weights[:, choice_k : choice_k + 1] * returned[
-            places[:, choice_k]
-        ].astype(jnp.float32)
-    return totals
+def core_index():
+    return lax.axis_index("tp_1")
+
+
+def partner(first, second):
+    me, core = lax.axis_index("sp"), core_index()
+    step_y = core * first + (1 - core) * second
+    step_x = (1 - core) * first + core * second
+    y = ((me >> 2) + step_y) & (SIDE - 1)
+    x = ((me & (SIDE - 1)) + step_x) & (SIDE - 1)
+    return {"sp": y * SIDE + x}
+
+
+def copies_to(sources, targets, send, recv, partners):
+    return [
+        pltpu.make_async_remote_copy(
+            source, target, send.at[i], recv.at[i],
+            device_id=device, device_id_type=pl.DeviceIdType.MESH,
+        )
+        for i, (source, target, device) in enumerate(zip(sources, targets, partners))
+    ]
+
+
+def start(copies):
+    for copy in copies:
+        copy.start()
+
+
+def arrived(copies):
+    for copy in copies:
+        copy.wait_recv()
+
+
+def experts_kernel(
+    rows_ref, table_ref, weight_hi, weight_lo, stream_ref, gate_hbm, up_hbm, down_hbm,
+    out_ref,
+    send_buf, there, answers, back_buf, gate_ref, up_ref, down_ref, load_sems, own_sems,
+    *sems,
+):
+    loads = [
+        pltpu.make_async_copy(hbm, ref, load_sems.at[i])
+        for i, (hbm, ref) in enumerate(((gate_hbm, gate_ref), (up_hbm, up_ref), (down_hbm, down_ref)))
+    ]
+    start(loads)
+    others = range(1, SIDE)
+    barrier = pltpu.get_barrier_semaphore()
+    for step in others:
+        for device in (partner(step, 0), partner(0, step)):
+            pl.semaphore_signal(
+                barrier, inc=1, device_id=device, device_id_type=pl.DeviceIdType.MESH
+            )
+
+    half = rows_ref.shape[0] // BLOCKS
+    width = rows_ref.shape[1]
+    slot = send_buf.shape[3]
+    slots = PARTNERS * slot
+    cols = 512
+
+    def pack(block):
+        @pl.loop(0, width // cols)
+        def _(c):
+            col = pl.ds(pl.multiple_of(c * cols, cols), cols)
+            packed = jnp.dot(
+                table_ref[block], rows_ref[pl.ds(block * half, half), col],
+                preferred_element_type=jnp.float32,
+            ).astype(jnp.bfloat16).reshape(SIDE, SIDE, slot, cols)
+            send_buf[block, :, :, :, col] = packed
+            there[block, pl.ds(0, SIDE), 0, :, col] = packed[0]
+
+    def experts(block):
+        @pl.loop(0, 2)
+        def _(m):
+            at = pl.ds(SIDE - 1 + m * 2, 2)
+            inputs = there[block, at].reshape(slots // 2, width)
+            gate = jnp.dot(inputs, gate_ref[...], preferred_element_type=jnp.float32)
+            up = jnp.dot(inputs, up_ref[...], preferred_element_type=jnp.float32)
+            hidden = (gate / (1.0 + jnp.exp(-gate)) * up).astype(jnp.bfloat16)
+            result = jnp.dot(hidden, down_ref[...], preferred_element_type=jnp.float32)
+            answers[block, at] = result.astype(jnp.bfloat16).reshape(2, SIDE, slot, width)
+
+    def combine(block):
+        @pl.loop(0, width // cols)
+        def _(c):
+            col = pl.ds(pl.multiple_of(c * cols, cols), cols)
+            own = pl.ds(block * half, half)
+            back = back_buf[block, :, :, :, col].reshape(slots, cols)
+            total = (
+                stream_ref[own, col]
+                + jnp.dot(weight_hi[block], back, preferred_element_type=jnp.float32)
+                + jnp.dot(weight_lo[block], back, preferred_element_type=jnp.float32)
+            )
+            out_ref[own, col] = total.astype(jnp.bfloat16)
+
+    def ahead(i, b):
+        return sems[2 * i].at[b], sems[2 * i + 1].at[b]
+
+    every = pl.ds(0, SIDE)
+    out_first = [
+        copies_to(
+            [send_buf.at[b, f] for f in others], [there.at[b, every, f] for f in others],
+            *ahead(0, b), [partner(f, 0) for f in others],
+        )
+        for b in range(BLOCKS)
+    ]
+    out_second = [
+        copies_to(
+            [there.at[b, g - 1] for g in others], [there.at[b, SIDE - 1 + g] for g in others],
+            *ahead(1, b), [partner(0, g) for g in others],
+        )
+        for b in range(BLOCKS)
+    ]
+    back_second = [
+        copies_to(
+            [answers.at[b, SIDE - 1 + g] for g in others], [answers.at[b, g - 1] for g in others],
+            *ahead(2, b), [partner(0, SIDE - g) for g in others],
+        )
+        for b in range(BLOCKS)
+    ]
+    back_first = [
+        copies_to(
+            [answers.at[b, every, f] for f in others], [back_buf.at[b, f] for f in others],
+            *ahead(3, b), [partner(SIDE - f, 0) for f in others],
+        )
+        for b in range(BLOCKS)
+    ]
+    own = [
+        pltpu.make_async_copy(answers.at[b, every, 0], back_buf.at[b, 0], own_sems.at[b])
+        for b in range(BLOCKS)
+    ]
+
+    pack(0)
+    pl.semaphore_wait(barrier, 2 * (SIDE - 1))
+    start(out_first[0])
+    pack(1)
+    start(out_first[1])
+    for b in range(BLOCKS):
+        arrived(out_first[b])
+        start(out_second[b])
+    for load in loads:
+        load.wait()
+    for b in range(BLOCKS):
+        arrived(out_second[b])
+        experts(b)
+        start(back_second[b])
+    for b in range(BLOCKS):
+        arrived(back_second[b])
+        start(back_first[b])
+        own[b].start()
+    for b in range(BLOCKS):
+        arrived(back_first[b])
+        own[b].wait()
+        combine(b)
+    for copies in (*out_first, *out_second, *back_second, *back_first):
+        for copy in copies:
+            copy.wait_send()
+
+
+def experts_call(rows, table, weight_hi, weight_lo, stream, w_gate, w_up, w_down):
+    count, width = rows.shape
+    slot = table.shape[1] // PARTNERS
+    ff = w_gate.shape[1]
+    vmem = pl.BlockSpec(memory_space=pltpu.VMEM)
+    hbm = pl.BlockSpec(memory_space=pl.ANY)
+    square = pltpu.VMEM((BLOCKS, SIDE, SIDE, slot, width), jnp.bfloat16)
+    longer = pltpu.VMEM((BLOCKS, 2 * SIDE - 1, SIDE, slot, width), jnp.bfloat16)
+    dma = pltpu.SemaphoreType.DMA
+    return pl.pallas_call(
+        experts_kernel,
+        out_shape=jax.ShapeDtypeStruct((count, width), jnp.bfloat16),
+        in_specs=[vmem] * 5 + [hbm] * 3,
+        out_specs=vmem,
+        scratch_shapes=[
+            square, longer, longer, square,
+            pltpu.VMEM((width, ff), jnp.bfloat16),
+            pltpu.VMEM((width, ff), jnp.bfloat16),
+            pltpu.VMEM((ff, width), jnp.bfloat16),
+            dma((3,)), dma((BLOCKS,)),
+            *[dma((BLOCKS, SIDE - 1))] * 8,
+        ],
+        compiler_params=pltpu.CompilerParams(
+            collective_id=1, has_side_effects=True, vmem_limit_bytes=56 * 1024 * 1024
+        ),
+        name="experts",
+    )(rows, table, weight_hi, weight_lo, stream, w_gate, w_up, w_down)
+
+
+def routing(route_ids, route_weight, slot):
+    rows = route_ids.shape[0]
+    half = rows // BLOCKS
+    me, core = lax.axis_index("sp"), core_index()
+    dy = ((route_ids >> 2) - (me >> 2)) & (SIDE - 1)
+    dx = (route_ids - me) & (SIDE - 1)
+    first = jnp.where(core == 0, dx, dy)
+    second = (jnp.where(core == 0, dy, dx) + SIDE - 1) & (SIDE - 1)
+    flat = (first * SIDE + second).reshape(BLOCKS, -1)
+    order = jnp.arange(flat.shape[1], dtype=jnp.int32)
+    same = (flat[:, :, None] == flat[:, None, :]) & (order[:, None] > order[None, :])
+    place = (flat * slot + jnp.sum(same.astype(jnp.int32), axis=2)).reshape(BLOCKS, half, -1)
+    targets = jnp.arange(PARTNERS * slot, dtype=jnp.int32)
+    table = jnp.any(targets[None, :, None, None] == place[:, None], axis=3).astype(jnp.bfloat16)
+    hit = (place[:, :, :, None] == targets).astype(jnp.float32)
+    weight = jnp.sum(hit * route_weight.reshape(BLOCKS, half, -1, 1), axis=2)
+    weight_hi = weight.astype(jnp.bfloat16)
+    weight_lo = (weight - weight_hi.astype(jnp.float32)).astype(jnp.bfloat16)
+    return table, weight_hi, weight_lo
 
 
 def body(
@@ -100,7 +290,6 @@
     head_normed = (by_head.reshape(channels, -1) * head_gain[:, None]).astype(jnp.bfloat16)
     by_row = exchange_by_chip(head_normed, ("tp_0", "tp_1"), (0, 1), 1, 0)
     rows = resid.shape[0]
-    width = resid.shape[1]
     mixed = lax.dot_general(
         by_row,
         lax.all_gather(out_proj, TP, axis=0, tiled=True),
@@ -111,35 +300,11 @@
     expert_in = (
         stream * lax.rsqrt(jnp.mean(stream * stream, axis=1, keepdims=True) + norm_eps) * norm_gain
     ).astype(jnp.bfloat16)
-    sp_count = lax.axis_size("sp")
-    local_experts = w_gate.shape[0]
-    experts_total = local_experts * sp_count
-    half = rows // 2
     slot = max(2, rows // 8)
-    parts = []
-    for block_no in range(2):
-        block_ids = route_ids[block_no * half : (block_no + 1) * half]
-        place = slot_places(block_ids, slot, experts_total)
-        send = pack_rows(
-            place, expert_in[block_no * half : (block_no + 1) * half], experts_total * slot
-        ).reshape(sp_count, local_experts, slot, width)
-        arrived = lax.all_to_all(send, "sp", split_axis=0, concat_axis=0, tiled=True)
-        gate_part = jnp.einsum(
-            "nesd,edf->nesf", arrived, w_gate, preferred_element_type=jnp.float32
-        )
-        up_part = jnp.einsum("nesd,edf->nesf", arrived, w_up, preferred_element_type=jnp.float32)
-        hidden = (jax.nn.silu(gate_part) * up_part).astype(jnp.bfloat16)
-        arrived = jnp.einsum(
-            "nesf,efd->nesd", hidden, w_down, preferred_element_type=jnp.float32
-        ).astype(jnp.bfloat16)
-        returned = lax.all_to_all(arrived, "sp", split_axis=0, concat_axis=0, tiled=True).reshape(
-            experts_total * slot, width
-        )
-        parts.append(
-            combine_rows(returned, place, route_weight[block_no * half : (block_no + 1) * half])
-        )
-    mixture = jnp.concatenate(parts, axis=0)
-    return (stream + mixture).astype(jnp.bfloat16)
+    table, weight_hi, weight_lo = routing(route_ids, route_weight, slot)
+    return experts_call(
+        expert_in, table, weight_hi, weight_lo, stream, w_gate[0], w_up[0], w_down[0]
+    )
 
 
 def solution(mesh):

time: 231 us -> 189 us (0.82)
  the two profiles are of different devices: /device:TPU:32 before, /device:TPU:18 now
where the time goes in v1:
time: 189 us; the launch traced here: 188 us
  Pallas kernels  111 us (59%)
  waiting for transfers between devices  28.9 us (15%)
  starting transfers between devices  15 us (8%)
  between operations  13.6 us (7%)
  other arithmetic  6.73 us (4%)
  local copies, waits for them, and re-layouts  4.92 us (3%)
  blocking collectives  4.25 us (2%)
  matrix products  3.57 us (2%)
    pallas_call x1, Pallas kernels, experts_call(): pl.pallas_call(experts_kernel, out_shape=jax.ShapeDtypeStruct((count, wid...  111 us
    all_to_all x1, waiting for transfers between devices, exchange_in_order(): lax.all_to_all(pieces, axes[k], split_axis=k, concat_axis=k, tiled=True)  19.1 us
    all_to_all x1, starting transfers between devices, exchange_in_order(): lax.all_to_all(pieces, axes[k], split_axis=k, concat_axis=k, tiled=True)  8.47 us
    all_gather x1, waiting for transfers between devices, body(): lax.all_gather(out_proj, TP, axis=0, tiled=True)  6.55 us
    ppermute x2, starting transfers between devices, shifted(): lax.ppermute(value, axis, [(source, source + steps) for source in range(l...  6.48 us
    all_to_all x1, blocking collectives, exchange_in_order(): lax.all_to_all(pieces, axes[k], split_axis=k, concat_axis=k, tiled=True)  4.25 us
  transfers between devices with their start and end apart: 4, of which 3 were waited for; matrix products, arithmetic and copies ran while one was open for 4% of the time, Pallas kernels for 0%

profile of v1, /device:TPU:18, one launch (start us, length us, event | category | flops | bytes accessed | tf_op | source)
XLA Modules:
  0.0 188.4 jit_solution(4105641612266828479)
XLA Ops:
  6.5 0.7 all-gather.2.cloned.1.call-update
  7.3 0.7 convert_element_type.48
  8.1 3.4 %collective-permute-start.1 = (f32[2]{0:T(128)S(1)}, f32[2]{0:T(128)S(1)}, u32[]{:S(2)}, u32[]{:S(2)}) collective-permute-start(f32[2]{0:T(128)S(1)} %slice.39), channel_id=1, source_target_pairs={{0,16},{16,32},{32,48},{48,64},{64,80},{80,96},{96,112},{112,128},... | collective-permute-start | bytes 32 | tf_op jit(solution)/shard_map/ppermute | solution.py:23
  11.5 1.3 convert_multiply_fusion
  12.8 0.1 slice.36
  12.8 3.1 %collective-permute-start = (f32[64,2]{1,0:T(8,128)S(1)}, f32[64,2]{1,0:T(8,128)S(1)}, u32[]{:S(2)}, u32[]{:S(2)}) collective-permute-start(f32[64,2]{1,0:T(8,128)S(1)} %slice.36), channel_id=1, source_target_pairs={{0,16},{16,32},{32,48},{48,64},{64,80},{80,96},{96,112},{112,128},... | collective-permute-start | bytes 1544 | tf_op jit(solution)/shard_map/ppermute | solution.py:23
  16.0 0.1 fusion.14
  16.1 2.6 %collective-permute-done = f32[64,2]{1,0:T(8,128)S(1)} collective-permute-done((f32[64,2]{1,0:T(8,128)S(1)}, f32[64,2]{1,0:T(8,128)S(1)}, u32[]{:S(2)}, u32[]{:S(2)}) %collective-permute-start) | collective-permute-done | bytes 544 | tf_op jit(solution)/shard_map/ppermute | solution.py:23
  18.6 0.7 multiply_reduce_fusion.1
  19.3 0.1 broadcast_multiply_fusion
  19.4 0.3 copy.45
  19.8 0.2 copy-done.7
  20.0 0.1 fusion.6
  20.2 1.0 copy.37
  21.1 8.5 %all-to-all-start = ((bf16[8,2,64,256]{3,2,1,0:T(8,128)(2,1)}), bf16[8,2,64,256]{3,2,1,0:T(8,128)(2,1)S(1)}, u32[]{:S(2)}, u32[]{:S(2)}) async-start(bf16[8,2,64,256]{3,2,1,0:T(8,128)(2,1)} %bitcast.4), calls=%async_computation | async-start | bytes 1048576 | tf_op jit(solution)/shard_map/all_to_all | solution.py:41
  29.6 0.1 copy.41
  29.7 0.1 eq.55
  29.9 0.2 convert_reduce_fusion
  30.2 0.1 reduce_sum.41
  30.3 0.1 copy.40
  30.6 0.2 fusion.9
  30.7 0.8 convert_element_type.54.table_ref
  31.5 0.2 select_reduce_fusion
  31.7 0.9 subtract_convert_fusion
  32.6 19.1 %all-to-all-done = bf16[8,2,64,256]{3,2,1,0:T(8,128)(2,1)S(1)} async-done(((bf16[8,2,64,256]{3,2,1,0:T(8,128)(2,1)}), bf16[8,2,64,256]{3,2,1,0:T(8,128)(2,1)S(1)}, u32[]{:S(2)}, u32[]{:S(2)}) %all-to-all-start) | async-done | bytes 524320 | tf_op jit(solution)/shard_map/all_to_all | solution.py:41
  51.7 4.2 %all_to_all.10 = bf16[8,2,64,256]{3,2,0,1:T(8,128)(2,1)S(1)} all-to-all(bf16[8,2,64,256]{3,2,0,1:T(8,128)(2,1)S(1)} %copy.38), channel_id=1, replica_groups=mesh['sp'=16,'tp_0'=8,'tp_1'=2] {'tp_1'}, dimensions={1} | all-to-all | bytes 1048576 | tf_op jit(solution)/shard_map/all_to_all | solution.py:41
  56.0 6.6 %all-gather.2.cloned.1.call-done = bf16[1024,2048]{1,0:T(8,128)(2,1)} async-done(((bf16[64,2048]{1,0:T(8,128)(2,1)}), bf16[1024,2048]{1,0:T(8,128)(2,1)}) %all-gather.2.cloned.1.call-update) | async-done | bytes 4194320 | tf_op jit(solution)/shard_map/all_gather | solution.py:295
  62.6 3.6 %multiply_reduce_fusion = (f32[256]{0:T(256)S(1)}, f32[256,2048]{1,0:T(8,128)S(1)}) fusion(bf16[1024,256]{1,0:T(8,128)(2,1)S(1)} %bitcast.22, bf16[1024,2048]{1,0:T(8,128)(2,1)} %all-gather.2.cloned.1.call-done, bf16[256,2048]{1,0:T(8,128)(2,1)S(1)} %copy-done.1), kind=kOutput, calls=%fused_computation.2 | convolution fusion | flops 1075838720 | bytes 7865344 | tf_op jit(solution)/shard_map/dot_general | solution.py:293
  66.2 1.4 multiply_convert_fusion.rows_ref
  67.6 0.2 copy-done
  67.8 111.5 %experts.1 = bf16[256,2048]{1,0:T(8,128)(2,1)} custom-call(bf16[256,2048]{1,0:T(8,128)(2,1)} %multiply_convert_fusion.rows_ref, bf16[2,512,128]{2,1,0:T(8,128)(2,1)} %convert_element_type.54.table_ref, bf16[2,128,512]{2,1,0:T(8,128)(2,1)} %get-tuple-element.6.weight_hi, bf16[2,128,512]{2,1,0:T(8,128)(2,1)} %get-tuple-element.5.weight_lo, ...), custom_call_target="tpu_custom_call" | custom-call | tf_op jit(solution)/shard_map/experts/pallas_call | solution.py:217
  179.3 2.3 %copy.47 = bf16[256,2048]{1,0:T(8,128)(2,1)} copy(bf16[256,2048]{1,0:T(8,128)(2,1)} %experts.1) | data formatting | bytes 2097152
  (26 shorter events, 0.3 us)
Async XLA Ops:
  6.5 9.4 %copy-start.6 = (f32[64,3]{0,1:T(4,128)S(1)}, f32[64,3]{0,1:T(4,128)}, u32[]{:S(2)}) copy-start(f32[64,3]{0,1:T(4,128)} %param.18) | copy-start | bytes 2308
  6.5 12.1 %copy-start.2 = (bf16[64,4096]{1,0:T(8,128)(2,1)S(1)}, bf16[64,4096]{1,0:T(8,128)(2,1)}, u32[]{:S(2)}) copy-start(bf16[64,4096]{1,0:T(8,128)(2,1)} %param.16) | copy-start | bytes 1572868
  6.5 56.0 %all-gather.2.cloned.1.call-start = ((), (), s32[]{:S(2)}) async-start(), calls=%async_computation.2 | async-start | bytes 4456448 | tf_op jit(solution)/shard_map/all_gather | solution.py:295
  8.1 7.9 %collective-permute-start.1 = (f32[2]{0:T(128)S(1)}, f32[2]{0:T(128)S(1)}, u32[]{:S(2)}, u32[]{:S(2)}) collective-permute-start(f32[2]{0:T(128)S(1)} %slice.39), channel_id=1, source_target_pairs={{0,16},{16,32},{32,48},{48,64},{64,80},{80,96},{96,112},{112,128},... | collective-permute-start | bytes 32 | tf_op jit(solution)/shard_map/ppermute | solution.py:23
  12.8 5.8 %collective-permute-start = (f32[64,2]{1,0:T(8,128)S(1)}, f32[64,2]{1,0:T(8,128)S(1)}, u32[]{:S(2)}, u32[]{:S(2)}) collective-permute-start(f32[64,2]{1,0:T(8,128)S(1)} %slice.36), channel_id=1, source_target_pairs={{0,16},{16,32},{32,48},{48,64},{64,80},{80,96},{96,112},{112,128},... | collective-permute-start | bytes 1544 | tf_op jit(solution)/shard_map/ppermute | solution.py:23
  19.3 0.7 copy-start.7
  20.0 9.6 %copy-start.5 = (s32[256,2]{0,1:T(2,128)S(1)}, s32[256,2]{0,1:T(2,128)}, u32[]{:S(2)}) copy-start(s32[256,2]{0,1:T(2,128)} %param.23) | copy-start | bytes 6148
  20.1 11.4 %copy-start.4 = (f32[256,2]{0,1:T(2,128)S(1)}, f32[256,2]{0,1:T(2,128)}, u32[]{:S(2)}) copy-start(f32[256,2]{0,1:T(2,128)} %param.24) | copy-start | bytes 6148
  21.1 30.6 %all-to-all-start = ((bf16[8,2,64,256]{3,2,1,0:T(8,128)(2,1)}), bf16[8,2,64,256]{3,2,1,0:T(8,128)(2,1)S(1)}, u32[]{:S(2)}, u32[]{:S(2)}) async-start(bf16[8,2,64,256]{3,2,1,0:T(8,128)(2,1)} %bitcast.4), calls=%async_computation | async-start | bytes 1048576 | tf_op jit(solution)/shard_map/all_to_all | solution.py:41
  31.7 30.8 %copy-start.1 = (bf16[256,2048]{1,0:T(8,128)(2,1)S(1)}, bf16[256,2048]{1,0:T(8,128)(2,1)}, u32[]{:S(2)}) copy-start(bf16[256,2048]{1,0:T(8,128)(2,1)} %param.21) | copy-start | bytes 3145732
  62.6 3.6 %copy-start.3 = (f32[2048]{0:T(1024)S(1)}, f32[2048]{0:T(1024)}, u32[]{:S(2)}) copy-start(f32[2048]{0:T(1024)} %param.22) | copy-start | bytes 24580
  66.1 1.7 copy-start
Sparse Core Ops, SparseCore 0:
  9.2 53.3 all-gather.1

commit v2 on v1

--- a/solution.py
+++ b/solution.py
@@ -8,6 +8,8 @@
 
 HEAD = 64
 TP = ("tp_0", "tp_1")
+LANES = 128
+HALO = LANES
 SP_TP = ("sp", "tp_0", "tp_1")
 SIDE = 4
 PARTNERS = SIDE * SIDE
@@ -17,56 +19,42 @@
 norm_eps = 1e-06
 
 
-def shifted(value, axis, steps):
-    count = lax.axis_size(axis)
-    leading, last = (max(0, -steps), min(count, count - steps))
-    return lax.ppermute(value, axis, [(source, source + steps) for source in range(leading, last)])
-
-
-def cut_along(array, dim, length):
-    before, after = (array.shape[:dim], array.shape[dim + 1 :])
-    return jnp.moveaxis(array.reshape(*before, length, -1, *after), dim, 0)
-
-
-def joined_along(pieces, dim):
-    dims = list(pieces.shape[1:])
-    dims[dim] *= pieces.shape[0]
-    return jnp.moveaxis(pieces, 0, dim).reshape(dims)
-
-
-def exchange_in_order(pieces, axes, sequence):
-    dims = [lax.axis_size(a) for a in axes]
-    pieces = pieces.reshape(*dims, *pieces.shape[1:])
-    for k in sequence:
-        pieces = lax.all_to_all(pieces, axes[k], split_axis=k, concat_axis=k, tiled=True)
-    return pieces.reshape(-1, *pieces.shape[len(axes) :])
-
-
-def exchange_by_chip(array, groups, sequence, split_dim, concat_dim):
-    length = lax.axis_size(groups[0]) * lax.axis_size(groups[1])
-    pieces = cut_along(array, split_dim, length)
-    return joined_along(exchange_in_order(pieces, groups, sequence), concat_dim)
-
-
 def core_index():
     return lax.axis_index("tp_1")
 
 
-def partner(first, second):
-    me, core = lax.axis_index("sp"), core_index()
+def place_at(core, first, second):
+    me = lax.axis_index("sp")
     step_y = core * first + (1 - core) * second
     step_x = (1 - core) * first + core * second
     y = ((me >> 2) + step_y) & (SIDE - 1)
     x = ((me & (SIDE - 1)) + step_x) & (SIDE - 1)
-    return {"sp": y * SIDE + x}
+    return y * SIDE + x
+
+
+def partner(first, second):
+    return {"sp": place_at(core_index(), first, second)}
+
+
+def tp_partner(steps):
+    depth = lax.axis_size("tp_0")
+    tp = (lax.axis_index("tp_0") * 2 + core_index() + steps) & (2 * depth - 1)
+    return {"tp_0": tp >> 1, "tp_1": tp & 1}
+
+
+def next_block(steps):
+    return {"sp": (lax.axis_index("sp") + steps) & (PARTNERS - 1)}
+
+
+def remote(source, target, send, recv, device):
+    return pltpu.make_async_remote_copy(
+        source, target, send, recv, device_id=device, device_id_type=pl.DeviceIdType.MESH
+    )
 
 
 def copies_to(sources, targets, send, recv, partners):
     return [
-        pltpu.make_async_remote_copy(
-            source, target, send.at[i], recv.at[i],
-            device_id=device, device_id_type=pl.DeviceIdType.MESH,
-        )
+        remote(source, target, send.at[i], recv.at[i], device)
         for i, (source, target, device) in enumerate(zip(sources, targets, partners))
     ]
 
@@ -81,24 +69,173 @@
         copy.wait_recv()
 
 
-def experts_kernel(
-    rows_ref, table_ref, weight_hi, weight_lo, stream_ref, gate_hbm, up_hbm, down_hbm,
+def layer_kernel(
+    taps_ref, head_ref, norm_ref, table_ref, weight_hi, weight_lo,
+    conv_hbm, gate_in_hbm, gate_out_hbm, docs_hbm, proj_hbm, resid_hbm,
+    gate_hbm, up_hbm, down_hbm,
     out_ref,
+    conv_buf, gate_in_buf, gate_out_buf, docs_buf, resid_buf, normed_buf, by_row, turned,
+    proj, rows_ref, stream_ref,
     send_buf, there, answers, back_buf, gate_ref, up_ref, down_ref, load_sems, own_sems,
+    halo_send, halo_recv, normed_send, normed_recv,
+    deep_send, deep_recv, row_send, row_recv, plane_send, plane_recv, pair_send, pair_recv,
     *sems,
 ):
-    loads = [
-        pltpu.make_async_copy(hbm, ref, load_sems.at[i])
-        for i, (hbm, ref) in enumerate(((gate_hbm, gate_ref), (up_hbm, up_ref), (down_hbm, down_ref)))
-    ]
-    start(loads)
+    me, core, layer = lax.axis_index("sp"), core_index(), lax.axis_index("tp_0")
+    depth = lax.axis_size("tp_0")
+    devices = 2 * depth
+    channels, length = gate_out_buf.shape
+    chunk = length // devices
     others = range(1, SIDE)
     barrier = pltpu.get_barrier_semaphore()
-    for step in others:
-        for device in (partner(step, 0), partner(0, step)):
-            pl.semaphore_signal(
-                barrier, inc=1, device_id=device, device_id_type=pl.DeviceIdType.MESH
-            )
+    greeted = [partner(step, 0) for step in others] + [partner(0, step) for step in others]
+    greeted += [next_block(1), next_block(-1)] + [tp_partner(k) for k in range(1, devices)]
+    for device in greeted:
+        pl.semaphore_signal(barrier, inc=1, device_id=device, device_id_type=pl.DeviceIdType.MESH)
+
+    body_at, halo_at = pl.ds(HALO, length), pl.ds(0, HALO)
+    tail_at = pl.ds(length, HALO)
+    own_shard = pl.ds(pl.multiple_of(layer * channels, channels), channels)
+    own_cols = pl.ds(pl.multiple_of(me * LANES, LANES), LANES)
+    pairs = (
+        (proj_hbm.at[:, own_cols], proj.at[core, me, own_shard]),
+        (conv_hbm, conv_buf.at[:, body_at]),
+        (gate_in_hbm, gate_in_buf.at[:, body_at]),
+        (docs_hbm, docs_buf.at[:, body_at]),
+        (gate_out_hbm, gate_out_buf),
+        (resid_hbm, resid_buf),
+        (gate_hbm, gate_ref),
+        (up_hbm, up_ref),
+        (down_hbm, down_ref),
+    )
+    loads = [
+        pltpu.make_async_copy(source, target, load_sems.at[i])
+        for i, (source, target) in enumerate(pairs)
+    ]
+    start(loads)
+    halo = [
+        remote(buf.at[:, tail_at], buf.at[:, halo_at], halo_send.at[i], halo_recv.at[i], next_block(1))
+        for i, buf in enumerate((conv_buf, gate_in_buf, docs_buf))
+    ]
+    deep = [
+        remote(
+            proj.at[core, me, own_shard], proj.at[core, me, own_shard],
+            deep_send.at[k - 1], deep_recv.at[k - 1], tp_partner(2 * k),
+        )
+        for k in range(1, depth)
+    ]
+    pl.semaphore_wait(barrier, len(greeted))
+    loads[0].wait()
+    start(deep)
+    for load in loads[1:4]:
+        load.wait()
+    start(halo)
+    loads[4].wait()
+
+    def normed_copy(k):
+        to = pl.multiple_of((core * depth + layer) * channels, channels)
+        return remote(
+            normed_buf.at[k], by_row.at[pl.ds(to, channels)], normed_send.at[k], normed_recv.at[k],
+            tp_partner(k),
+        )
+
+    def convolved(k):
+        j = (layer * 2 + core + k) & (devices - 1)
+
+        @pl.when(j == 0)
+        def _():
+            arrived(halo)
+
+        wide = pl.ds(pl.multiple_of(j * chunk, chunk), chunk + HALO)
+        gated = conv_buf[:, wide].astype(jnp.float32) * gate_in_buf[:, wide].astype(jnp.float32)
+        docs = jnp.broadcast_to(docs_buf[:, wide], (8, chunk + HALO))
+        lane = lax.broadcasted_iota(jnp.int32, docs.shape, 1)
+        docs = jnp.where((j == 0) & (me == 0) & (lane < HALO), -1, docs)
+        same_one = (pltpu.roll(docs, 1, 1) == docs).astype(jnp.float32)[:1, HALO:]
+        same_two = (pltpu.roll(docs, 2, 1) == docs).astype(jnp.float32)[:1, HALO:]
+        conv = (
+            taps_ref[:, 2:3] * gated[:, HALO:]
+            + taps_ref[:, 1:2] * (pltpu.roll(gated, 1, 1)[:, HALO:] * same_one)
+            + taps_ref[:, 0:1] * (pltpu.roll(gated, 2, 1)[:, HALO:] * same_two)
+        )
+        own = pl.ds(pl.multiple_of(j * chunk, chunk), chunk)
+        value = gate_out_buf[:, own].astype(jnp.float32) * conv
+        scale = lax.rsqrt(jnp.mean(value * value, axis=0, keepdims=True) + norm_eps)
+        return (value * scale * head_ref[...]).astype(jnp.bfloat16)
+
+    @pl.loop(0, devices - 1)
+    def _(i):
+        k = devices // 2 + jnp.where((i & 1) == 1, -((i + 1) >> 1), i >> 1)
+        normed_buf[k] = convolved(k)
+        normed_copy(k).start()
+
+    by_row[pl.ds(pl.multiple_of((core * depth + layer) * channels, channels), channels)] = convolved(0)
+
+    def piece(f, g, c=core):
+        return proj.at[c, place_at(c, f, g)]
+
+    def pair_copy(f, g, c):
+        return remote(
+            piece(f, g, c), piece(f, g, c),
+            pair_send.at[f & (SIDE - 1), g & (SIDE - 1)], pair_recv.at[f & (SIDE - 1), g & (SIDE - 1)],
+            {"tp_1": 1 - core},
+        )
+
+    row = [
+        remote(piece(0, 0), piece(0, 0), row_send.at[f - 1], row_recv.at[f - 1], partner(f, 0))
+        for f in others
+    ]
+    plane = {
+        (f, g): remote(
+            piece(-f, 0), piece(-f, 0), plane_send.at[f, g - 1], plane_recv.at[f, g - 1], partner(0, g)
+        )
+        for f in range(SIDE) for g in others
+    }
+    arrived(deep)
+    start(row)
+    start([plane[0, g] for g in others])
+    pair_copy(0, 0, core).start()
+    for f in (1, 3, 2):
+        row[f - 1].wait_recv()
+        start([plane[f, g] for g in others])
+        pair_copy(-f, 0, core).start()
+
+    for k in range(1, devices):
+        normed_copy(k).wait_recv()
+    turned[...] = by_row[...].T
+    for g in (1, 3, 2):
+        for f in range(SIDE):
+            plane[f, g].wait_recv()
+            pair_copy(-f, -g, core).start()
+    for f in range(SIDE):
+        for g in range(SIDE):
+            pair_copy(-f, -g, 1 - core).wait_recv()
+    loads[5].wait()
+
+    count = resid_buf.shape[0]
+    step = 2
+
+    def project(i, total):
+        col = pl.ds(pl.multiple_of(i * step * LANES, step * LANES), step * LANES)
+        mixed = jnp.zeros((count, step * LANES), jnp.float32)
+        for c in range(2):
+            right = jnp.concatenate([proj[c, i * step + n] for n in range(step)], axis=1)
+            left = turned[:, pl.ds(c * depth * channels, depth * channels)]
+            mixed = mixed + jnp.dot(left, right, preferred_element_type=jnp.float32)
+        value = resid_buf[:, col].astype(jnp.float32) + mixed
+        stream_ref[:, col] = value
+        return total + value * value
+
+    total = lax.fori_loop(
+        0, PARTNERS // step, project, jnp.zeros((count, step * LANES), jnp.float32)
+    )
+    mean = jnp.sum(total, axis=1, keepdims=True) / (PARTNERS * LANES)
+    scale = lax.rsqrt(mean + norm_eps)
+
+    @pl.loop(0, PARTNERS // step)
+    def _(i):
+        col = pl.ds(pl.multiple_of(i * step * LANES, step * LANES), step * LANES)
+        rows_ref[:, col] = (stream_ref[:, col] * scale * norm_ref[:, col]).astype(jnp.bfloat16)
 
     half = rows_ref.shape[0] // BLOCKS
     width = rows_ref.shape[1]
@@ -179,14 +316,13 @@
     ]
 
     pack(0)
-    pl.semaphore_wait(barrier, 2 * (SIDE - 1))
     start(out_first[0])
     pack(1)
     start(out_first[1])
     for b in range(BLOCKS):
         arrived(out_first[b])
         start(out_second[b])
-    for load in loads:
+    for load in loads[6:]:
         load.wait()
     for b in range(BLOCKS):
         arrived(out_second[b])
@@ -200,38 +336,64 @@
         arrived(back_first[b])
         own[b].wait()
         combine(b)
-    for copies in (*out_first, *out_second, *back_second, *back_first):
+    sent = [*halo, *deep, *row, *plane.values(), *[normed_copy(k) for k in range(1, devices)]]
+    sent += [pair_copy(-f, -g, core) for f in range(SIDE) for g in range(SIDE)]
+    for copies in (sent, *out_first, *out_second, *back_second, *back_first):
         for copy in copies:
             copy.wait_send()
 
 
-def experts_call(rows, table, weight_hi, weight_lo, stream, w_gate, w_up, w_down):
-    count, width = rows.shape
+def layer_call(
+    conv_in, in_gate, out_gate, docs, taps, head_gain, out_proj, resid, norm_gain,
+    table, weight_hi, weight_lo, w_gate, w_up, w_down,
+):
+    count, width = resid.shape
+    channels, length = conv_in.shape
     slot = table.shape[1] // PARTNERS
     ff = w_gate.shape[1]
+    depth = lax.axis_size("tp_0")
+    devices = 2 * depth
+    bf16 = jnp.bfloat16
     vmem = pl.BlockSpec(memory_space=pltpu.VMEM)
     hbm = pl.BlockSpec(memory_space=pl.ANY)
-    square = pltpu.VMEM((BLOCKS, SIDE, SIDE, slot, width), jnp.bfloat16)
-    longer = pltpu.VMEM((BLOCKS, 2 * SIDE - 1, SIDE, slot, width), jnp.bfloat16)
+    square = pltpu.VMEM((BLOCKS, SIDE, SIDE, slot, width), bf16)
+    longer = pltpu.VMEM((BLOCKS, 2 * SIDE - 1, SIDE, slot, width), bf16)
     dma = pltpu.SemaphoreType.DMA
     return pl.pallas_call(
-        experts_kernel,
-        out_shape=jax.ShapeDtypeStruct((count, width), jnp.bfloat16),
-        in_specs=[vmem] * 5 + [hbm] * 3,
+        layer_kernel,
+        out_shape=jax.ShapeDtypeStruct((count, width), bf16),
+        in_specs=[vmem] * 6 + [hbm] * 9,
         out_specs=vmem,
         scratch_shapes=[
+            pltpu.VMEM((channels, HALO + length), bf16),
+            pltpu.VMEM((channels, HALO + length), bf16),
+            pltpu.VMEM((channels, length), bf16),
+            pltpu.VMEM((1, HALO + length), jnp.int32),
+            pltpu.VMEM((count, width), bf16),
+            pltpu.VMEM((devices, channels, length // devices), bf16),
+            pltpu.VMEM((devices * channels, count), bf16),
+            pltpu.VMEM((count, devices * channels), bf16),
+            pltpu.VMEM((2, PARTNERS, depth * channels, width // PARTNERS), bf16),
+            pltpu.VMEM((count, width), bf16),
+            pltpu.VMEM((count, width), jnp.float32),
             square, longer, longer, square,
-            pltpu.VMEM((width, ff), jnp.bfloat16),
-            pltpu.VMEM((width, ff), jnp.bfloat16),
-            pltpu.VMEM((ff, width), jnp.bfloat16),
-            dma((3,)), dma((BLOCKS,)),
+            pltpu.VMEM((width, ff), bf16),
+            pltpu.VMEM((width, ff), bf16),
+            pltpu.VMEM((ff, width), bf16),
+            dma((9,)), dma((BLOCKS,)),
+            dma((3,)), dma((3,)), dma((devices,)), dma((devices,)),
+            dma((depth - 1,)), dma((depth - 1,)), dma((SIDE - 1,)), dma((SIDE - 1,)),
+            dma((SIDE, SIDE - 1)), dma((SIDE, SIDE - 1)), dma((SIDE, SIDE)), dma((SIDE, SIDE)),
             *[dma((BLOCKS, SIDE - 1))] * 8,
         ],
         compiler_params=pltpu.CompilerParams(
-            collective_id=1, has_side_effects=True, vmem_limit_bytes=56 * 1024 * 1024
+            collective_id=1, has_side_effects=True, vmem_limit_bytes=60 * 1024 * 1024
         ),
-        name="experts",
-    )(rows, table, weight_hi, weight_lo, stream, w_gate, w_up, w_down)
+        name="layer",
+    )(
+        taps, head_gain, norm_gain, table, weight_hi, weight_lo,
+        conv_in, in_gate, out_gate, docs, out_proj, resid, w_gate, w_up, w_down,
+    )
 
 
 def routing(route_ids, route_weight, slot):
@@ -271,39 +433,12 @@
     w_up,
     w_down,
 ):
-    gated_in = in_gate.astype(jnp.float32) * conv_in.astype(jnp.float32)
-    doc_value = doc_ids.astype(jnp.float32)
-    earlier_in, earlier_doc = shifted((gated_in[:, -2:], doc_value[-2:]), "sp", 1)
-    padded_in = jnp.concatenate([earlier_in, gated_in], axis=1)
-    padded_doc = jnp.concatenate([earlier_doc, doc_value])
-    same_one = (padded_doc[1:-1] == doc_value).astype(jnp.float32)
-    same_two = (padded_doc[:-2] == doc_value).astype(jnp.float32)
-    conv_out = (
-        conv_taps[:, 2:3] * gated_in
-        + conv_taps[:, 1:2] * (padded_in[:, 1:-1] * same_one)
-        + conv_taps[:, 0:1] * (padded_in[:, :-2] * same_two)
-    )
-    gated_out = out_gate.astype(jnp.float32) * conv_out
-    channels = gated_out.shape[0]
-    by_head = gated_out.reshape(channels // HEAD, HEAD, -1)
-    by_head = by_head * lax.rsqrt(jnp.mean(by_head * by_head, axis=1, keepdims=True) + norm_eps)
-    head_normed = (by_head.reshape(channels, -1) * head_gain[:, None]).astype(jnp.bfloat16)
-    by_row = exchange_by_chip(head_normed, ("tp_0", "tp_1"), (0, 1), 1, 0)
-    rows = resid.shape[0]
-    mixed = lax.dot_general(
-        by_row,
-        lax.all_gather(out_proj, TP, axis=0, tiled=True),
-        (((0,), (0,)), ((), ())),
-        preferred_element_type=jnp.float32,
-    )
-    stream = resid.astype(jnp.float32) + mixed
-    expert_in = (
-        stream * lax.rsqrt(jnp.mean(stream * stream, axis=1, keepdims=True) + norm_eps) * norm_gain
-    ).astype(jnp.bfloat16)
-    slot = max(2, rows // 8)
+    slot = max(2, resid.shape[0] // 8)
     table, weight_hi, weight_lo = routing(route_ids, route_weight, slot)
-    return experts_call(
-        expert_in, table, weight_hi, weight_lo, stream, w_gate[0], w_up[0], w_down[0]
+    return layer_call(
+        conv_in, in_gate, out_gate, doc_ids.reshape(1, -1), conv_taps, head_gain.reshape(-1, 1),
+        out_proj, resid, norm_gain.reshape(1, -1), table, weight_hi, weight_lo,
+        w_gate[0], w_up[0], w_down[0],
     )
 
 

time: 189 us -> 161 us (0.85)
  the two profiles are of different devices: /device:TPU:18 before, /device:TPU:203 now
where the time goes in v2:
time: 161 us
  Pallas kernels  152 us (94%)
  local copies, waits for them, and re-layouts  5.65 us (4%)
  other arithmetic  3.7 us (2%)
    pallas_call x1, Pallas kernels, layer_call(): pl.pallas_call(layer_kernel, out_shape=jax.ShapeDtypeStruct((count, width...  152 us
    unnamed x2, local copies, waits for them, and re-layouts  3.67 us

profile of v2, /device:TPU:203, one launch (start us, length us, event | category | flops | bytes accessed | tf_op | source)
XLA Modules:
  0.0 161.0 jit_solution(6266264675572009623)
XLA Ops:
  0.0 0.7 broadcast_multiply_fusion
  0.7 1.4 copy.30.taps_ref
  2.1 1.3 copy.31.head_ref
  3.4 0.1 copy.25
  3.6 0.1 copy.26
  3.7 0.1 eq.47
  3.9 0.3 convert_reduce_fusion
  4.1 0.1 reduce_sum.21
  4.3 0.1 copy.27
  4.4 0.2 fusion
  4.6 0.8 convert_element_type.17.table_ref
  5.3 0.9 select_reduce_fusion
  6.2 0.9 subtract_convert_fusion
  7.1 151.6 %layer.1 = bf16[256,2048]{1,0:T(8,128)(2,1)} custom-call(f32[64,3]{1,0:T(8,128)} %copy.30.taps_ref, f32[64,1]{1,0:T(8,128)} %copy.31.head_ref, f32[1,2048]{1,0:T(1,128)} %bitcast.13, bf16[2,512,128]{2,1,0:T(8,128)(2,1)} %convert_element_type.17.table_ref, bf16[2,128,512]{2,1,0:T(8,128)(2,1)} %get-tuple-element.6.weight_hi, ...), custom_call_target="tpu_custom_call" | custom-call | tf_op jit(solution)/shard_map/layer/pallas_call | solution.py:362
  158.7 2.3 %copy.33 = bf16[256,2048]{1,0:T(8,128)(2,1)} copy(bf16[256,2048]{1,0:T(8,128)(2,1)} %layer.1) | data formatting | bytes 2097152
  (2 shorter events, 0.0 us)

commit v3 on v2

--- a/solution.py
+++ b/solution.py
@@ -70,12 +70,12 @@
 
 
 def layer_kernel(
-    taps_ref, head_ref, norm_ref, table_ref, weight_hi, weight_lo,
+    taps_ref, head_ref, norm_ref, ids_ref, share_ref,
     conv_hbm, gate_in_hbm, gate_out_hbm, docs_hbm, proj_hbm, resid_hbm,
     gate_hbm, up_hbm, down_hbm,
     out_ref,
     conv_buf, gate_in_buf, gate_out_buf, docs_buf, resid_buf, normed_buf, by_row, turned,
-    proj, rows_ref, stream_ref,
+    proj, rows_ref, stream_ref, squares, table_ref, weight_hi, weight_lo,
     send_buf, there, answers, back_buf, gate_ref, up_ref, down_ref, load_sems, own_sems,
     halo_send, halo_recv, normed_send, normed_recv,
     deep_send, deep_recv, row_send, row_recv, plane_send, plane_recv, pair_send, pair_recv,
@@ -124,13 +124,10 @@
         )
         for k in range(1, depth)
     ]
-    pl.semaphore_wait(barrier, len(greeted))
-    loads[0].wait()
-    start(deep)
-    for load in loads[1:4]:
-        load.wait()
-    start(halo)
-    loads[4].wait()
+    def column(row):
+        square = (row.shape[1], row.shape[1])
+        diagonal = lax.broadcasted_iota(jnp.int32, square, 0) == lax.broadcasted_iota(jnp.int32, square, 1)
+        return jnp.sum(jnp.where(diagonal, jnp.broadcast_to(row, square), 0.0), axis=1, keepdims=True)
 
     def normed_copy(k):
         to = pl.multiple_of((core * depth + layer) * channels, channels)
@@ -139,13 +136,11 @@
             tp_partner(k),
         )
 
-    def convolved(k):
+    tap_0, tap_1, tap_2 = (column(taps_ref[i : i + 1, :]) for i in range(3))
+    gain = column(head_ref[...])
+
+    def convolve(k):
         j = (layer * 2 + core + k) & (devices - 1)
-
-        @pl.when(j == 0)
-        def _():
-            arrived(halo)
-
         wide = pl.ds(pl.multiple_of(j * chunk, chunk), chunk + HALO)
         gated = conv_buf[:, wide].astype(jnp.float32) * gate_in_buf[:, wide].astype(jnp.float32)
         docs = jnp.broadcast_to(docs_buf[:, wide], (8, chunk + HALO))
@@ -154,116 +149,162 @@
         same_one = (pltpu.roll(docs, 1, 1) == docs).astype(jnp.float32)[:1, HALO:]
         same_two = (pltpu.roll(docs, 2, 1) == docs).astype(jnp.float32)[:1, HALO:]
         conv = (
-            taps_ref[:, 2:3] * gated[:, HALO:]
-            + taps_ref[:, 1:2] * (pltpu.roll(gated, 1, 1)[:, HALO:] * same_one)
-            + taps_ref[:, 0:1] * (pltpu.roll(gated, 2, 1)[:, HALO:] * same_two)
+            tap_2 * gated[:, HALO:]
+            + tap_1 * (pltpu.roll(gated, 1, 1)[:, HALO:] * same_one)
+            + tap_0 * (pltpu.roll(gated, 2, 1)[:, HALO:] * same_two)
         )
         own = pl.ds(pl.multiple_of(j * chunk, chunk), chunk)
         value = gate_out_buf[:, own].astype(jnp.float32) * conv
         scale = lax.rsqrt(jnp.mean(value * value, axis=0, keepdims=True) + norm_eps)
-        return (value * scale * head_ref[...]).astype(jnp.bfloat16)
+        normed_buf[k] = (value * scale * gain).astype(jnp.bfloat16)
+
+    for load in loads[1:5]:
+        load.wait()
+    first_chunk = (devices - layer * 2 - core) & (devices - 1)
+
+    @pl.loop(1, devices)
+    def _(i):
+        convolve((first_chunk + i) & (devices - 1))
+
+    pl.semaphore_wait(barrier, len(greeted))
+    start(halo)
+    loads[0].wait()
+    start(deep)
+
+    half = resid_buf.shape[0] // BLOCKS
+    slot = send_buf.shape[3]
+    slots = PARTNERS * slot
+    dy = ((ids_ref[...] >> 2) - (me >> 2)) & (SIDE - 1)
+    dx = (ids_ref[...] - me) & (SIDE - 1)
+    f_of = dx * (1 - core) + dy * core
+    g_of = (dy * (1 - core) + dx * core + SIDE - 1) & (SIDE - 1)
+    group = f_of * SIDE + g_of
+    earlier = (
+        lax.broadcasted_iota(jnp.int32, (half, half), 0) < lax.broadcasted_iota(jnp.int32, (half, half), 1)
+    ).astype(jnp.bfloat16)
+    for b in range(BLOCKS):
+        counted = jnp.zeros((PARTNERS, 1), jnp.float32)
+        marked = jnp.zeros((slots, half), jnp.float32)
+        shares = jnp.zeros((slots, half), jnp.float32)
+        for choice in range(2):
+            mine = group[choice : choice + 1, b * half : (b + 1) * half]
+            marks = (lax.broadcasted_iota(jnp.int32, (PARTNERS, half), 0) == mine).astype(jnp.float32)
+            before = counted + jnp.dot(
+                marks.astype(jnp.bfloat16), earlier, preferred_element_type=jnp.float32
+            )
+            place = mine.astype(jnp.float32) * slot + jnp.sum(marks * before, axis=0, keepdims=True)
+            counted = counted + jnp.sum(marks, axis=1, keepdims=True)
+            hit = lax.broadcasted_iota(jnp.int32, (slots, half), 0).astype(jnp.float32) == place
+            marked = jnp.where(hit, 1.0, marked)
+            shares = jnp.where(hit, share_ref[choice : choice + 1, b * half : (b + 1) * half], shares)
+        table_ref[b] = marked.astype(jnp.bfloat16)
+        by_position = shares.T
+        high = by_position.astype(jnp.bfloat16)
+        weight_hi[b] = high
+        weight_lo[b] = (by_position - high.astype(jnp.float32)).astype(jnp.bfloat16)
+
+    arrived(halo)
+    convolve(first_chunk)
+
+    def piece(f, g, c):
+        return proj.at[c, place_at(c, f, g)]
+
+    def pair_copy(f, g, c):
+        at = (f & (SIDE - 1), g & (SIDE - 1))
+        return remote(piece(f, g, c), piece(f, g, c), pair_send.at[at], pair_recv.at[at], {"tp_1": 1 - core})
+
+    def row_copy(f):
+        return remote(
+            piece(0, 0, core), piece(0, 0, core), row_send.at[f - 1], row_recv.at[f - 1], partner(f, 0)
+        )
+
+    def plane_copy(f, g):
+        return remote(
+            piece(-f, 0, core), piece(-f, 0, core), plane_send.at[f, g - 1], plane_recv.at[f, g - 1],
+            partner(0, g),
+        )
+
+    arrived(deep)
+    start([row_copy(f) for f in (1, 3, 2)])
+    start([plane_copy(0, g) for g in (1, 3, 2)])
+    pair_copy(0, 0, core).start()
 
     @pl.loop(0, devices - 1)
     def _(i):
-        k = devices // 2 + jnp.where((i & 1) == 1, -((i + 1) >> 1), i >> 1)
-        normed_buf[k] = convolved(k)
-        normed_copy(k).start()
-
-    by_row[pl.ds(pl.multiple_of((core * depth + layer) * channels, channels), channels)] = convolved(0)
-
-    def piece(f, g, c=core):
-        return proj.at[c, place_at(c, f, g)]
-
-    def pair_copy(f, g, c):
-        return remote(
-            piece(f, g, c), piece(f, g, c),
-            pair_send.at[f & (SIDE - 1), g & (SIDE - 1)], pair_recv.at[f & (SIDE - 1), g & (SIDE - 1)],
-            {"tp_1": 1 - core},
-        )
-
-    row = [
-        remote(piece(0, 0), piece(0, 0), row_send.at[f - 1], row_recv.at[f - 1], partner(f, 0))
-        for f in others
-    ]
-    plane = {
-        (f, g): remote(
-            piece(-f, 0), piece(-f, 0), plane_send.at[f, g - 1], plane_recv.at[f, g - 1], partner(0, g)
-        )
-        for f in range(SIDE) for g in others
-    }
-    arrived(deep)
-    start(row)
-    start([plane[0, g] for g in others])
-    pair_copy(0, 0, core).start()
+        normed_copy(devices // 2 + jnp.where((i & 1) == 1, -((i + 1) >> 1), i >> 1)).start()
+
+    by_row[pl.ds(pl.multiple_of((core * depth + layer) * channels, channels), channels)] = normed_buf[0]
     for f in (1, 3, 2):
-        row[f - 1].wait_recv()
-        start([plane[f, g] for g in others])
+        row_copy(f).wait_recv()
+        start([plane_copy(f, g) for g in (1, 3, 2)])
         pair_copy(-f, 0, core).start()
-
-    for k in range(1, devices):
+    loads[5].wait()
+    squares[...] = jnp.zeros_like(squares)
+
+    @pl.loop(1, devices)
+    def _(k):
         normed_copy(k).wait_recv()
+
     turned[...] = by_row[...].T
-    for g in (1, 3, 2):
-        for f in range(SIDE):
-            plane[f, g].wait_recv()
-            pair_copy(-f, -g, core).start()
-    for f in range(SIDE):
-        for g in range(SIDE):
-            pair_copy(-f, -g, 1 - core).wait_recv()
-    loads[5].wait()
-
-    count = resid_buf.shape[0]
-    step = 2
-
-    def project(i, total):
-        col = pl.ds(pl.multiple_of(i * step * LANES, step * LANES), step * LANES)
-        mixed = jnp.zeros((count, step * LANES), jnp.float32)
-        for c in range(2):
-            right = jnp.concatenate([proj[c, i * step + n] for n in range(step)], axis=1)
-            left = turned[:, pl.ds(c * depth * channels, depth * channels)]
-            mixed = mixed + jnp.dot(left, right, preferred_element_type=jnp.float32)
-        value = resid_buf[:, col].astype(jnp.float32) + mixed
-        stream_ref[:, col] = value
-        return total + value * value
-
-    total = lax.fori_loop(
-        0, PARTNERS // step, project, jnp.zeros((count, step * LANES), jnp.float32)
-    )
-    mean = jnp.sum(total, axis=1, keepdims=True) / (PARTNERS * LANES)
+
+    def ordered(i):
+        return i ^ (i >> 1)
+
+    for n in range(SIDE):
+        if n:
+
+            @pl.loop(0, SIDE)
+            def _(i):
+                plane_copy(ordered(i), ordered(n)).wait_recv()
+                pair_copy(-ordered(i), -ordered(n), core).start()
+
+        @pl.loop(0, 2 * n + 1)
+        def _(m):
+            f, g = ordered(jnp.minimum(m, n)), ordered(jnp.minimum(n, 2 * n - m))
+            pair_copy(-g, -f, 1 - core).wait_recv()
+            at = place_at(core, -f, -g)
+            col = pl.ds(pl.multiple_of(at * LANES, LANES), LANES)
+            mixed = jnp.dot(
+                turned[:, : depth * channels], proj[0, at], preferred_element_type=jnp.float32
+            ) + jnp.dot(turned[:, depth * channels :], proj[1, at], preferred_element_type=jnp.float32)
+            value = resid_buf[:, col].astype(jnp.float32) + mixed
+            stream_ref[:, col] = value
+            squares[...] += value * value
+
+    mean = jnp.sum(squares[...], axis=1, keepdims=True) / (PARTNERS * LANES)
     scale = lax.rsqrt(mean + norm_eps)
-
-    @pl.loop(0, PARTNERS // step)
+    step = 2 * LANES
+
+    @pl.loop(0, PARTNERS * LANES // step)
     def _(i):
-        col = pl.ds(pl.multiple_of(i * step * LANES, step * LANES), step * LANES)
+        col = pl.ds(pl.multiple_of(i * step, step), step)
         rows_ref[:, col] = (stream_ref[:, col] * scale * norm_ref[:, col]).astype(jnp.bfloat16)
 
-    half = rows_ref.shape[0] // BLOCKS
     width = rows_ref.shape[1]
-    slot = send_buf.shape[3]
-    slots = PARTNERS * slot
     cols = 512
 
-    def pack(block):
+    def pack(block, f):
         @pl.loop(0, width // cols)
         def _(c):
             col = pl.ds(pl.multiple_of(c * cols, cols), cols)
             packed = jnp.dot(
-                table_ref[block], rows_ref[pl.ds(block * half, half), col],
+                table_ref[block, pl.ds(f * SIDE * slot, SIDE * slot)],
+                rows_ref[pl.ds(block * half, half), col],
                 preferred_element_type=jnp.float32,
-            ).astype(jnp.bfloat16).reshape(SIDE, SIDE, slot, cols)
-            send_buf[block, :, :, :, col] = packed
-            there[block, pl.ds(0, SIDE), 0, :, col] = packed[0]
-
-    def experts(block):
-        @pl.loop(0, 2)
-        def _(m):
-            at = pl.ds(SIDE - 1 + m * 2, 2)
-            inputs = there[block, at].reshape(slots // 2, width)
-            gate = jnp.dot(inputs, gate_ref[...], preferred_element_type=jnp.float32)
-            up = jnp.dot(inputs, up_ref[...], preferred_element_type=jnp.float32)
-            hidden = (gate / (1.0 + jnp.exp(-gate)) * up).astype(jnp.bfloat16)
-            result = jnp.dot(hidden, down_ref[...], preferred_element_type=jnp.float32)
-            answers[block, at] = result.astype(jnp.bfloat16).reshape(2, SIDE, slot, width)
+            ).astype(jnp.bfloat16).reshape(SIDE, slot, cols)
+            if f:
+                send_buf[block, f, :, :, col] = packed
+            else:
+                there[block, pl.ds(0, SIDE), 0, :, col] = packed
+
+    def experts(block, m):
+        at = pl.ds(SIDE - 1 + m * 2, 2)
+        inputs = there[block, at].reshape(slots // 2, width)
+        gate = jnp.dot(inputs, gate_ref[...], preferred_element_type=jnp.float32)
+        up = jnp.dot(inputs, up_ref[...], preferred_element_type=jnp.float32)
+        hidden = (gate / (1.0 + jnp.exp(-gate)) * up).astype(jnp.bfloat16)
+        result = jnp.dot(hidden, down_ref[...], preferred_element_type=jnp.float32)
+        answers[block, at] = result.astype(jnp.bfloat16).reshape(2, SIDE, slot, width)
 
     def combine(block):
         @pl.loop(0, width // cols)
@@ -315,41 +356,68 @@
         for b in range(BLOCKS)
     ]
 
-    pack(0)
-    start(out_first[0])
-    pack(1)
-    start(out_first[1])
-    for b in range(BLOCKS):
-        arrived(out_first[b])
-        start(out_second[b])
+    pack(0, 2)
+    pack(0, 1)
+    out_first[0][1].start()
+    pack(0, 3)
+    out_first[0][0].start()
+    pack(0, 0)
+    out_first[0][2].start()
+    arrived(out_first[0])
+    start([out_second[0][i] for i in (1, 0, 2)])
+    pack(1, 2)
+    pack(1, 1)
+    out_first[1][1].start()
+    pack(1, 3)
+    out_first[1][0].start()
+    pack(1, 0)
+    out_first[1][2].start()
+    arrived(out_first[1])
+    start([out_second[1][i] for i in (1, 0, 2)])
     for load in loads[6:]:
         load.wait()
     for b in range(BLOCKS):
-        arrived(out_second[b])
-        experts(b)
-        start(back_second[b])
+        arrived(out_second[b][1:])
+        experts(b, 1)
+        start(back_second[b][1:])
+        arrived(out_second[b][:1])
+        experts(b, 0)
+        start(back_second[b][:1])
     for b in range(BLOCKS):
         arrived(back_second[b])
-        start(back_first[b])
+        start([back_first[b][i] for i in (1, 0, 2)])
         own[b].start()
     for b in range(BLOCKS):
         arrived(back_first[b])
         own[b].wait()
         combine(b)
-    sent = [*halo, *deep, *row, *plane.values(), *[normed_copy(k) for k in range(1, devices)]]
-    sent += [pair_copy(-f, -g, core) for f in range(SIDE) for g in range(SIDE)]
-    for copies in (sent, *out_first, *out_second, *back_second, *back_first):
+
+    @pl.loop(1, devices)
+    def _(k):
+        normed_copy(k).wait_send()
+
+    @pl.loop(0, PARTNERS)
+    def _(i):
+        f, g = i & (SIDE - 1), i >> 2
+        pair_copy(-f, -g, core).wait_send()
+
+        @pl.when(g > 0)
+        def _():
+            plane_copy(f, g).wait_send()
+
+    for copies in (halo, deep, [row_copy(f) for f in others], *out_first, *out_second, *back_second, *back_first):
         for copy in copies:
             copy.wait_send()
 
 
 def layer_call(
     conv_in, in_gate, out_gate, docs, taps, head_gain, out_proj, resid, norm_gain,
-    table, weight_hi, weight_lo, w_gate, w_up, w_down,
+    route_ids, route_weight, w_gate, w_up, w_down,
 ):
     count, width = resid.shape
     channels, length = conv_in.shape
-    slot = table.shape[1] // PARTNERS
+    slot = max(2, count // 8)
+    half = count // BLOCKS
     ff = w_gate.shape[1]
     depth = lax.axis_size("tp_0")
     devices = 2 * depth
@@ -362,7 +430,7 @@
     return pl.pallas_call(
         layer_kernel,
         out_shape=jax.ShapeDtypeStruct((count, width), bf16),
-        in_specs=[vmem] * 6 + [hbm] * 9,
+        in_specs=[vmem] * 5 + [hbm] * 9,
         out_specs=vmem,
         scratch_shapes=[
             pltpu.VMEM((channels, HALO + length), bf16),
@@ -376,6 +444,10 @@
             pltpu.VMEM((2, PARTNERS, depth * channels, width // PARTNERS), bf16),
             pltpu.VMEM((count, width), bf16),
             pltpu.VMEM((count, width), jnp.float32),
+            pltpu.VMEM((count, LANES), jnp.float32),
+            pltpu.VMEM((BLOCKS, PARTNERS * slot, half), bf16),
+            pltpu.VMEM((BLOCKS, half, PARTNERS * slot), bf16),
+            pltpu.VMEM((BLOCKS, half, PARTNERS * slot), bf16),
             square, longer, longer, square,
             pltpu.VMEM((width, ff), bf16),
             pltpu.VMEM((width, ff), bf16),
@@ -391,30 +463,9 @@
         ),
         name="layer",
     )(
-        taps, head_gain, norm_gain, table, weight_hi, weight_lo,
+        taps, head_gain, norm_gain, route_ids, route_weight,
         conv_in, in_gate, out_gate, docs, out_proj, resid, w_gate, w_up, w_down,
     )
-
-
-def routing(route_ids, route_weight, slot):
-    rows = route_ids.shape[0]
-    half = rows // BLOCKS
-    me, core = lax.axis_index("sp"), core_index()
-    dy = ((route_ids >> 2) - (me >> 2)) & (SIDE - 1)
-    dx = (route_ids - me) & (SIDE - 1)
-    first = jnp.where(core == 0, dx, dy)
-    second = (jnp.where(core == 0, dy, dx) + SIDE - 1) & (SIDE - 1)
-    flat = (first * SIDE + second).reshape(BLOCKS, -1)
-    order = jnp.arange(flat.shape[1], dtype=jnp.int32)
-    same = (flat[:, :, None] == flat[:, None, :]) & (order[:, None] > order[None, :])
-    place = (flat * slot + jnp.sum(same.astype(jnp.int32), axis=2)).reshape(BLOCKS, half, -1)
-    targets = jnp.arange(PARTNERS * slot, dtype=jnp.int32)
-    table = jnp.any(targets[None, :, None, None] == place[:, None], axis=3).astype(jnp.bfloat16)
-    hit = (place[:, :, :, None] == targets).astype(jnp.float32)
-    weight = jnp.sum(hit * route_weight.reshape(BLOCKS, half, -1, 1), axis=2)
-    weight_hi = weight.astype(jnp.bfloat16)
-    weight_lo = (weight - weight_hi.astype(jnp.float32)).astype(jnp.bfloat16)
-    return table, weight_hi, weight_lo
 
 
 def body(
@@ -433,11 +484,9 @@
     w_up,
     w_down,
 ):
-    slot = max(2, resid.shape[0] // 8)
-    table, weight_hi, weight_lo = routing(route_ids, route_weight, slot)
     return layer_call(
-        conv_in, in_gate, out_gate, doc_ids.reshape(1, -1), conv_taps, head_gain.reshape(-1, 1),
-        out_proj, resid, norm_gain.reshape(1, -1), table, weight_hi, weight_lo,
+        conv_in, in_gate, out_gate, doc_ids.reshape(1, -1), conv_taps.T, head_gain.reshape(1, -1),
+        out_proj, resid, norm_gain.reshape(1, -1), route_ids.T, route_weight.T,
         w_gate[0], w_up[0], w_down[0],
     )
 

time: 161 us -> 148 us (0.919)
  the two profiles are of different devices: /device:TPU:203 before, /device:TPU:32 now
where the time goes in v3:
time: 148 us; the launch traced here: 145 us
  Pallas kernels  143 us (97%)
  local copies, waits for them, and re-layouts  2.3 us (2%)
    pallas_call x1, Pallas kernels, layer_call(): pl.pallas_call(layer_kernel, out_shape=jax.ShapeDtypeStruct((count, width...  143 us

profile of v3, /device:TPU:32, one launch (start us, length us, event | category | flops | bytes accessed | tf_op | source)
XLA Modules:
  0.0 145.4 jit_solution(4615581087791996669)
XLA Ops:
  0.0 143.1 %layer.1 = bf16[256,2048]{1,0:T(8,128)(2,1)} custom-call(f32[3,64]{1,0:T(4,128)} %bitcast.14, f32[1,64]{1,0:T(1,128)} %bitcast.17, f32[1,2048]{1,0:T(1,128)} %bitcast.13, s32[2,256]{1,0:T(2,128)} %bitcast.15, f32[2,256]{1,0:T(2,128)} %bitcast.16, bf16[64,4096]{1,0:T(8,128)(2,1)} %conv_hbm.1, bf16[64,4096]{1,0:T(8,128)(2,1)} %gate_in_hbm.1, ...), custom_call_target="tpu_custom_call" | custom-call | tf_op jit(solution)/shard_map/layer/pallas_call | solution.py:430
  143.1 2.3 %copy.16 = bf16[256,2048]{1,0:T(8,128)(2,1)} copy(bf16[256,2048]{1,0:T(8,128)(2,1)} %layer.1) | data formatting | bytes 2097152

commit v4 on v3

--- a/solution.py
+++ b/solution.py
@@ -225,8 +225,8 @@
         )
 
     arrived(deep)
-    start([row_copy(f) for f in (1, 3, 2)])
-    start([plane_copy(0, g) for g in (1, 3, 2)])
+    start([row_copy(f) for f in (2, 1, 3)])
+    start([plane_copy(0, g) for g in (2, 1, 3)])
     pair_copy(0, 0, core).start()
 
     @pl.loop(0, devices - 1)
@@ -236,7 +236,7 @@
     by_row[pl.ds(pl.multiple_of((core * depth + layer) * channels, channels), channels)] = normed_buf[0]
     for f in (1, 3, 2):
         row_copy(f).wait_recv()
-        start([plane_copy(f, g) for g in (1, 3, 2)])
+        start([plane_copy(f, g) for g in (2, 1, 3)])
         pair_copy(-f, 0, core).start()
     loads[5].wait()
     squares[...] = jnp.zeros_like(squares)
@@ -376,21 +376,21 @@
     start([out_second[1][i] for i in (1, 0, 2)])
     for load in loads[6:]:
         load.wait()
-    for b in range(BLOCKS):
-        arrived(out_second[b][1:])
-        experts(b, 1)
-        start(back_second[b][1:])
-        arrived(out_second[b][:1])
-        experts(b, 0)
-        start(back_second[b][:1])
+    arrived(out_second[0])
+    experts(0, 1)
+    experts(0, 0)
+    start([back_second[0][i] for i in (1, 0, 2)])
+    arrived(out_second[1])
+    experts(1, 1)
+    experts(1, 0)
+    start([back_second[1][i] for i in (1, 0, 2)])
     for b in range(BLOCKS):
         arrived(back_second[b])
         start([back_first[b][i] for i in (1, 0, 2)])
         own[b].start()
-    for b in range(BLOCKS):
-        arrived(back_first[b])
-        own[b].wait()
-        combine(b)
+    arrived(back_first[0])
+    own[0].wait()
+    combine(0)
 
     @pl.loop(1, devices)
     def _(k):
@@ -405,7 +405,14 @@
         def _():
             plane_copy(f, g).wait_send()
 
-    for copies in (halo, deep, [row_copy(f) for f in others], *out_first, *out_second, *back_second, *back_first):
+    for copies in (halo, deep, [row_copy(f) for f in others], *out_first, *out_second):
+        for copy in copies:
+            copy.wait_send()
+
+    arrived(back_first[1])
+    own[1].wait()
+    combine(1)
+    for copies in (*back_second, *back_first):
         for copy in copies:
             copy.wait_send()
 

time: 148 us -> 148 us (level)
  no operation moved by 1% of the time
where the time goes in v4:
time: 148 us; the launch traced here: 146 us
  Pallas kernels  144 us (97%)
  local copies, waits for them, and re-layouts  2.3 us (2%)
    pallas_call x1, Pallas kernels, layer_call(): pl.pallas_call(layer_kernel, out_shape=jax.ShapeDtypeStruct((count, width...  144 us

profile of v4, /device:TPU:32, one launch (start us, length us, event | category | flops | bytes accessed | tf_op | source)
XLA Modules:
  0.0 146.4 jit_solution(4166803734521450336)
XLA Ops:
  0.0 144.1 %layer.1 = bf16[256,2048]{1,0:T(8,128)(2,1)} custom-call(f32[3,64]{1,0:T(4,128)} %bitcast.14, f32[1,64]{1,0:T(1,128)} %bitcast.17, f32[1,2048]{1,0:T(1,128)} %bitcast.13, s32[2,256]{1,0:T(2,128)} %bitcast.15, f32[2,256]{1,0:T(2,128)} %bitcast.16, bf16[64,4096]{1,0:T(8,128)(2,1)} %conv_hbm.1, bf16[64,4096]{1,0:T(8,128)(2,1)} %gate_in_hbm.1, ...), custom_call_target="tpu_custom_call" | custom-call | tf_op jit(solution)/shard_map/layer/pallas_call | solution.py:437
  144.1 2.3 %copy.16 = bf16[256,2048]{1,0:T(8,128)(2,1)} copy(bf16[256,2048]{1,0:T(8,128)(2,1)} %layer.1) | data formatting | bytes 2097152
